TPU v7x, 32 devices: a whole 2x2x4 slice. The times are simulated.
32 devices in a mesh: grp: 2 (over y), sp: 4 (over z), tp: 4 (over x, core).
Axes of the slice: x: 2, y: 2, z: 4, core: 2. Of those that a mesh axis runs over, the one named last changes fastest.
Arguments:
- tokens: bfloat16 [8, 1024, 4096], P(('grp', 'tp'), 'sp'), parts along dimension 0, may hold values from -8 to 8, as said below
- offsets: int32 [8], P(('grp', 'tp')), parts along dimension 0, may hold values from 0 to 4095
- in_gain: float32 [4096], replicated, may hold values from 0.1 to 1.9
- w_latent: bfloat16 [4096, 1024], P('sp'), may hold values from -0.09375 to 0.09375
- w_rope_key: bfloat16 [4096, 32], replicated, may hold values from -0.09375 to 0.09375
- kv_gain: float32 [1024], replicated, may hold values from 0.1 to 1.9
- w_up_key: bfloat16 [1024, 2048], P(None, 'tp'), may hold values from -0.1875 to 0.1875
- w_up_value: bfloat16 [1024, 2048], P(None, 'tp'), may hold values from -0.1875 to 0.1875
- q_nope: bfloat16 [8, 2048], P(('grp', 'sp'), 'tp'), parts along dimension 0, may hold values from -300 to 300, as said below
- q_rope: bfloat16 [8, 1024], P(('grp', 'sp'), 'tp'), parts along dimension 0, may hold values from -16 to 16
Outputs:
- keys: bfloat16 [8, 1024, 2048], P(('grp', 'sp'), None, 'tp'), parts along dimension 0
- values: bfloat16 [8, 1024, 2048], P(('grp', 'sp'), None, 'tp'), parts along dimension 0
- rope_keys: bfloat16 [8, 32, 1024], P(('grp', 'sp')), parts along dimension 0
- read: bfloat16 [8, 2048], P(('grp', 'sp'), 'tp'), parts along dimension 0
There are 2 independent parts, one for each index of `grp`. A program takes and returns all parts, laid end to end along the dimension named above; an argument that names none is the same for every part. Nothing has to cross between parts.
Inputs may be any that keep to these rules, and one draw needn't show every extreme that they name: `tokens`: entries of the layer's input. `q_nope`: entries of the first decoding token's queries.
All inputs are finite; a program needn't handle non-finite values.
Results may differ from a plain program's by a relative error of at most 0.02.
Values may be sent and summed in bfloat16 or wider, within the bound.
A program may use at most 128 MiB of HBM per device.

v0:
```python
import functools

import jax
import jax.numpy as jnp
import numpy as np
from jax import lax
from jax.experimental import pallas as pl
from jax.experimental.pallas import tpu as pltpu
from jax.sharding import PartitionSpec as P

HEAD = 64
ROPE = 32
LANES = 128
CORES = 2
GROUPS = 4
LAGS = (3, 6, 7)
HOP = 3


EPS = 1e-06
MESH = pl.DeviceIdType.MESH


def gather_kernel(
    n_grp,
    n_sp,
    n_tp,
    groups,
    tok_hbm,
    w_hbm,
    w_rope_hbm,
    in_gain,
    offsets,
    inverse,
    lat_out,
    rope_out,
    tok,
    w_own,
    w_rope,
    normed,
    wbuf,
    acc,
    own,
    own_rope,
    transit,
    local_sem,
    own_send,
    z_send,
    z_recv,
    a_send,
    a_recv,
    b_send,
    b_recv,
    c_send,
    c_recv,
    l_send,
    t_send,
    t_recv,
    x_send,
    d_send,
    l_recv,
):
    n_x = n_tp // CORES
    prompts, rows = own.shape[1:3]
    depth, cols = w_own.shape
    width = cols // groups
    chunk = wbuf.shape[5]
    y, z, t = lax.axis_index("grp"), lax.axis_index("sp"), lax.axis_index("tp")
    x, core = t // CORES, t % CORES
    rank = (core * n_x + x) * n_grp + y
    half = n_x // 2

    def tp_of(x_to, core_to):
        return {"tp": x_to * CORES + core_to}

    x_peers = [lax.rem(x + k, n_x) for k in range(1, n_x)]
    y_peers = [lax.rem(y + k, n_grp) for k in range(1, n_grp)]
    z_peers = [lax.rem(z + k, n_sp) for k in range(1, n_sp)]

    fetch_tok = pltpu.make_async_copy(tok_hbm, tok, local_sem.at[0])
    fetch_w = pltpu.make_async_copy(w_hbm, w_own, local_sem.at[1])
    fetch_rope = pltpu.make_async_copy(w_rope_hbm, w_rope, local_sem.at[2])
    fetch_tok.start()
    fetch_w.start()
    fetch_rope.start()

    barrier = pltpu.get_barrier_semaphore()
    targets = (
        [tp_of(p, core) for p in x_peers]
        + [{"grp": p} for p in y_peers]
        + [{"sp": p} for p in z_peers]
        + [tp_of(x, 1 - core)]
    )
    for target in targets:
        pl.semaphore_signal(barrier, inc=1, device_id=target, device_id_type=MESH)
    pl.semaphore_wait(barrier, len(targets))

    finish = []

    def remote(src, dst, send, recv, device):
        return pltpu.make_async_remote_copy(
            src_ref=src,
            dst_ref=dst,
            send_sem=send,
            recv_sem=recv,
            device_id=device,
            device_id_type=MESH,
        )

    def arrived(ref, recv):
        remote(ref, ref, recv, recv, tp_of(x, 1 - core)).wait_recv()

    units = [(g, d) for g in range(groups) for d in range(1, n_sp)]
    above = n_sp - 1 - z
    both = jnp.minimum(z, above)

    def shard(d):
        paired = d <= 2 * both
        hop = jnp.where(paired, (d + 1) // 2, d - both)
        up = jnp.where(paired, d % 2 == 1, above > z)
        return jnp.where(up, z + hop, z - hop), up

    shards = {d: shard(d) for d in range(1, n_sp)}

    def own_z(g):
        for side, ahead, exists in ((0, z + 1, z + 1 < n_sp), (1, z + n_sp - 1, z > 0)):
            copy = remote(
                w_hbm.at[pl.ds(rank * chunk, chunk), pl.ds(g * width, width)],
                wbuf.at[g, z, core, x, y],
                own_send.at[g, side],
                z_recv.at[g, z],
                {"sp": lax.rem(ahead, n_sp)},
            )
            pl.when(exists)(copy.start)
            finish.append(lambda exists=exists, copy=copy: pl.when(exists)(copy.wait_send))

    def pass_z(u):
        g, d = units[u]
        s, up = shards[d]
        exists = jnp.where(up, z > 0, z + 1 < n_sp)
        ahead = jnp.where(up, z + n_sp - 1, z + 1)
        copy = remote(
            block_a(u),
            block_a(u),
            z_send.at[u],
            z_recv.at[g, s],
            {"sp": lax.rem(ahead, n_sp)},
        )
        pl.when(exists)(copy.start)
        finish.append(lambda: pl.when(exists)(copy.wait_send))

    def x_first(u):
        return u % 3 > 0

    def spread(u, src, send, recv, along_x):
        peers = x_peers if along_x else y_peers
        for k, peer in enumerate(peers):
            copy = remote(
                src,
                src,
                send.at[u, k],
                recv.at[u, k],
                tp_of(peer, core) if along_x else {"grp": peer},
            )
            copy.start()
            finish.append(copy.wait_send)

    def block_a(u):
        g, d = units[u]
        return wbuf.at[g, shards[d][0], core, x, y]

    def block_b(u):
        g, d = units[u]
        if x_first(u):
            return wbuf.at[g, shards[d][0], core, :, y]
        return wbuf.at[g, shards[d][0], core, x]

    def stage_a(u):
        arrived(block_a(u), z_recv.at[units[u][0], shards[units[u][1]][0]])
        pass_z(u)
        spread(u, block_a(u), a_send, a_recv, x_first(u))

    def stage_b(u):
        g, _ = units[u]
        for k in range(len(x_peers if x_first(u) else y_peers)):
            arrived(block_a(u), a_recv.at[u, k])
        spread(u, block_b(u), b_send, b_recv, not x_first(u))

    def stage_c(u):
        g, d = units[u]
        for k in range(len(y_peers if x_first(u) else x_peers)):
            arrived(block_b(u), b_recv.at[u, k])
        ref = wbuf.at[g, shards[d][0], core]
        copy = remote(ref, ref, c_send.at[u], c_recv.at[u], tp_of(x, 1 - core))
        copy.start()
        finish.append(copy.wait_send)

    def stage_dot(u):
        g, d = units[u]
        arrived(wbuf.at[g, shards[d][0], core], c_recv.at[u])
        s, _ = shards[d]
        weight = wbuf[g, s].reshape(depth, width)
        acc[g] += jnp.dot(
            normed[s], weight, preferred_element_type=jnp.float32
        )

    def crossing(m):
        return m % 2 == 1 and m < groups and n_x % 2 == 0

    def slot(m, s):
        if m == 0:
            return rope_out.at[s]
        return lat_out.at[m - 1, s]

    def mine(m, i):
        return own_rope.at[i] if m == 0 else own.at[m - 1, i]

    swapped = lax.rem(x + half, n_x) * CORES + core

    def stage_l(m):
        for i in range(prompts):
            home = t * prompts + i
            if crossing(m):
                copy = remote(
                    mine(m, i), transit.at[m, i], l_send.at[m, i], t_recv.at[m, i], {"tp": swapped}
                )
            else:
                copy = remote(
                    mine(m, i), slot(m, z), l_send.at[m, i], l_recv.at[m, z], {"sp": home}
                )
            pl.when(home != z)(copy.start)
            finish.append(lambda home=home, copy=copy: pl.when(home != z)(copy.wait_send))

    def stage_t(m):
        for i in range(prompts):
            home = swapped * prompts + i
            copy = remote(
                transit.at[m, i], slot(m, z), t_send.at[m, i], l_recv.at[m, z], {"sp": home}
            )

            def pass_on(m=m, i=i, copy=copy):
                arrived(transit.at[m, i], t_recv.at[m, i])
                copy.start()

            pl.when(home != z)(pass_on)
            finish.append(lambda home=home, copy=copy: pl.when(home != z)(copy.wait_send))

    owner = z // prompts

    def entry(m, e):
        x_in, core_in = owner // CORES, owner % CORES
        if crossing(m) and e > 0:
            x_in = lax.rem(x_in + half, n_x)
        return x_in, core_in

    def partner_copy(m, e):
        s = lax.rem(z + e, n_sp)
        return remote(slot(m, s), slot(m, s), d_send.at[m, e], l_recv.at[m, s], tp_of(x, 1 - core))

    def stage_x(m, e):
        s = lax.rem(z + e, n_sp)
        x_in, core_in = entry(m, e)
        here = (x == x_in) & (core == core_in)
        copies = [
            remote(slot(m, s), slot(m, s), x_send.at[m, e, k], l_recv.at[m, s], tp_of(peer, core))
            for k, peer in enumerate(x_peers)
        ]

        def enter():
            if e > 0:
                arrived(slot(m, s), l_recv.at[m, s])
            for copy in copies:
                copy.start()
            partner_copy(m, e).start()

        pl.when(here)(enter)

        def drain():
            for copy in copies:
                copy.wait_send()
            partner_copy(m, e).wait_send()

        finish.append(lambda: pl.when(here)(drain))

    def stage_d(m, e):
        s = lax.rem(z + e, n_sp)
        x_in, core_in = entry(m, e)
        here = (x != x_in) & (core == core_in)

        def hand():
            arrived(slot(m, s), l_recv.at[m, s])
            partner_copy(m, e).start()

        pl.when(here)(hand)
        finish.append(lambda: pl.when(here)(partner_copy(m, e).wait_send))

    def stage_end(m, e):
        s = lax.rem(z + e, n_sp)
        _, core_in = entry(m, e)
        pl.when(core != core_in)(lambda: arrived(slot(m, s), l_recv.at[m, s]))

    def finalize(m, value):
        value = value.reshape(prompts, rows, value.shape[-1])
        for i in range(prompts):
            mine(m, i)[...] = value[i]

            def keep(i=i):
                slot(m, z)[...] = value[i]

            pl.when(t * prompts + i == z)(keep)

    for g in range(groups):
        own_z(g)

    step_rows, pieces = 16, 4

    def norm(r, carry):
        at = pl.ds(pl.multiple_of(r * step_rows, step_rows), step_rows)
        wide = tok[at, :].astype(jnp.float32)
        scale = lax.rsqrt(jnp.mean(wide * wide, axis=-1, keepdims=True) + EPS)
        out = (wide * scale * in_gain[...]).astype(jnp.bfloat16)
        for b in range(n_sp):
            normed[b, at, :] = out[:, b * depth : (b + 1) * depth]
        return carry

    def norm_piece(k):
        turns = prompts * rows // step_rows // pieces
        lax.fori_loop(k * turns, (k + 1) * turns, norm, 0)

    work = {}

    def at_step(step, fn, *args):
        work.setdefault(step, []).append((fn, args))

    def own_dot(g):
        acc[g] = jnp.dot(
            normed[z], w_own[:, g * width : (g + 1) * width], preferred_element_type=jnp.float32
        )

    def rope_item():
        fetch_rope.wait()
        raw = jnp.zeros((prompts * rows, ROPE), jnp.float32)
        for b in range(n_sp):
            raw += lax.dot_general(
                normed[b],
                w_rope[:, b * depth : (b + 1) * depth],
                (((1,), (1,)), ((), ())),
                preferred_element_type=jnp.float32,
            )
        half_rope = ROPE // 2
        blank = jnp.zeros((prompts * rows, LANES - ROPE), jnp.float32)
        lane = lax.broadcasted_iota(jnp.int32, (rows, LANES), 1)
        index = lax.broadcasted_iota(jnp.int32, (rows, LANES), 0)
        plain = jnp.concatenate([raw, blank], axis=1)
        other = jnp.concatenate([raw[:, half_rope:], raw[:, :half_rope], blank], axis=1)
        turned = []
        for i in range(prompts):
            position = offsets[i] + z * rows + index
            angle = position.astype(jnp.float32) * inverse[...]
            sine = jnp.sin(angle)
            sine = jnp.where(lane < half_rope, -sine, sine)
            at = slice(i * rows, (i + 1) * rows)
            turned.append(plain[at] * jnp.cos(angle) + other[at] * sine)
        finalize(0, jnp.concatenate(turned, axis=0).astype(jnp.bfloat16))

    def group_item(g):
        finalize(g + 1, acc[g].astype(jnp.bfloat16))

    def route(m, step):
        at_step(step, stage_l, m)
        if crossing(m):
            step += HOP
            at_step(step, stage_t, m)
        for e in range(n_sp):
            at_step(step + HOP, stage_x, m, e)
        for e in range(n_sp):
            at_step(step + 2 * HOP, stage_d, m, e)

    lag_b, lag_c, lag_dot = LAGS
    for u, (g, d) in enumerate(units):
        at_step(u, stage_a, u)
        at_step(u + lag_b, stage_b, u)
        at_step(u + lag_c, stage_c, u)
    at_step(0, fetch_tok.wait)
    for k in range(pieces):
        at_step(k, norm_piece, k)
    at_step(pieces, fetch_w.wait)
    at_step(pieces, rope_item)
    route(0, pieces)
    for u, (g, d) in enumerate(units):
        step = max(u + lag_dot, pieces)
        if d == 1:
            at_step(step, own_dot, g)
        at_step(step, stage_dot, u)
        if d == n_sp - 1:
            at_step(step, group_item, g)
            route(g + 1, step)

    for step in sorted(work):
        for fn, args in work[step]:
            fn(*args)
    for m in range(groups + 1):
        for e in range(n_sp):
            stage_end(m, e)
    for fn in finish:
        fn()


def gather_latent(tokens, w_latent, w_rope, in_gain, offsets, inverse):
    prompts, rows, width = tokens.shape
    n_grp, n_sp, n_tp = (lax.axis_size(a) for a in ("grp", "sp", "tp"))
    n_x = n_tp // CORES
    depth, cols = w_latent.shape
    groups = max(1, GROUPS * 3 // (n_sp - 1) // 4 * 4)
    part = cols // groups
    chunk = depth // (n_grp * n_tp)
    total = prompts * rows
    units = groups * (n_sp - 1)
    peers = max(n_x, n_grp) - 1
    items = groups + 1
    bf16, f32 = jnp.bfloat16, jnp.float32
    dma = pltpu.SemaphoreType.DMA
    vmem = pl.BlockSpec(memory_space=pltpu.VMEM)
    hbm = pl.BlockSpec(memory_space=pl.ANY)
    return pl.pallas_call(
        functools.partial(gather_kernel, n_grp, n_sp, n_tp, groups),
        out_shape=(
            jax.ShapeDtypeStruct((groups, n_sp, rows, part), bf16),
            jax.ShapeDtypeStruct((n_sp, rows, LANES), bf16),
        ),
        in_specs=[hbm, hbm, hbm, vmem, pl.BlockSpec(memory_space=pltpu.SMEM), vmem],
        out_specs=(vmem, vmem),
        scratch_shapes=[
            pltpu.VMEM((total, width), bf16),
            pltpu.VMEM((depth, cols), bf16),
            pltpu.VMEM((ROPE, width), bf16),
            pltpu.VMEM((n_sp, total, depth), bf16),
            pltpu.VMEM((groups, n_sp, CORES, n_x, n_grp, chunk, part), bf16),
            pltpu.VMEM((groups, total, part), f32),
            pltpu.VMEM((groups, prompts, rows, part), bf16),
            pltpu.VMEM((prompts, rows, LANES), bf16),
            pltpu.VMEM((items, prompts, rows, part), bf16),
            dma((3,)),
            dma((groups, 2)),
            dma((units,)),
            dma((groups, n_sp)),
            dma((units, peers)),
            dma((units, peers)),
            dma((units, peers)),
            dma((units, peers)),
            dma((units,)),
            dma((units,)),
            dma((items, prompts)),
            dma((items, prompts)),
            dma((items, prompts)),
            dma((items, n_sp, max(n_x - 1, 1))),
            dma((items, n_sp)),
            dma((items, n_sp)),
        ],
        compiler_params=pltpu.CompilerParams(
            collective_id=0, has_side_effects=True, vmem_limit_bytes=60 * 1024 * 1024
        ),
    )(tokens.reshape(total, width), w_latent, w_rope, in_gain, offsets, inverse)


def cache_kernel(
    n_blocks,
    latent_ref,
    gain_ref,
    wk_ref,
    wv_ref,
    q_nope_ref,
    q_rope_ref,
    rope_ref,
    keys_ref,
    values_ref,
    rope_keys_ref,
    read_ref,
    scores,
    held,
):
    b = pl.program_id(0)
    heads = scores.shape[1]

    def per_head(row, size):
        wide = jnp.broadcast_to(row.astype(jnp.float32), (heads, heads * size))
        head = lax.broadcasted_iota(jnp.int32, wide.shape, 0)
        lane = lax.broadcasted_iota(jnp.int32, wide.shape, 1)
        return jnp.where((lane >= head * size) & (lane < head * size + size), wide, 0.0)

    query = per_head(q_nope_ref[...], HEAD).astype(jnp.bfloat16)
    spread = (heads * ROPE, LANES)
    fold = lax.broadcasted_iota(jnp.int32, spread, 0) % ROPE == lax.broadcasted_iota(
        jnp.int32, spread, 1
    )
    rotary_q = jnp.dot(
        per_head(q_rope_ref[...], ROPE).astype(jnp.bfloat16),
        jnp.where(fold, 1.0, 0.0).astype(jnp.bfloat16),
        preferred_element_type=jnp.float32,
    ).astype(jnp.bfloat16)
    parts = [latent_ref[g, 0] for g in range(latent_ref.shape[0])]
    raw = jnp.concatenate(parts, axis=1).astype(jnp.float32)
    scale = lax.rsqrt(jnp.mean(raw * raw, axis=-1, keepdims=True) + EPS)
    latent = (raw * scale * gain_ref[...]).astype(jnp.bfloat16)
    keys = jnp.dot(latent, wk_ref[...], preferred_element_type=jnp.float32).astype(jnp.bfloat16)
    keys_ref[...] = keys
    values = jnp.dot(latent, wv_ref[...], preferred_element_type=jnp.float32).astype(jnp.bfloat16)
    values_ref[...] = values
    held[b] = values
    rope = rope_ref[0]
    rope_keys_ref[...] = rope.astype(jnp.float32).T[:ROPE].astype(jnp.bfloat16)
    across = (((1,), (1,)), ((), ()))
    part = lax.dot_general(query, keys, across, preferred_element_type=jnp.float32)
    part += lax.dot_general(rotary_q, rope, across, preferred_element_type=jnp.float32)
    scores[b] = part / jnp.sqrt(jnp.float32(HEAD + ROPE))

    @pl.when(b == n_blocks - 1)
    def _():
        every = scores[...]
        peak = jnp.max(jnp.max(every, axis=-1, keepdims=True), axis=0, keepdims=True)
        expo = jnp.exp(every - peak)
        total = jnp.sum(jnp.sum(expo, axis=-1, keepdims=True), axis=0, keepdims=True)
        weights = (expo / total).astype(jnp.bfloat16)
        out = jnp.dot(weights[0], held[0], preferred_element_type=jnp.float32)
        for i in range(1, n_blocks):
            out += jnp.dot(weights[i], held[i], preferred_element_type=jnp.float32)
        head = lax.broadcasted_iota(jnp.int32, out.shape, 0)
        lane = lax.broadcasted_iota(jnp.int32, out.shape, 1)
        picked = jnp.where((lane >= head * HEAD) & (lane < head * HEAD + HEAD), out, 0.0)
        read_ref[...] = jnp.sum(picked, axis=0, keepdims=True).astype(jnp.bfloat16)


def fill_cache(latent, kv_gain, w_up_key, w_up_value, q_nope, q_rope, rope):
    groups, n_blocks, rows, part = latent.shape
    cols = groups * part
    out_cols = w_up_key.shape[1]
    heads = out_cols // HEAD
    length = n_blocks * rows
    whole = lambda shape: pl.BlockSpec(shape, lambda b: (0,) * len(shape))
    return pl.pallas_call(
        functools.partial(cache_kernel, n_blocks),
        grid=(n_blocks,),
        out_shape=(
            jax.ShapeDtypeStruct((length, out_cols), jnp.bfloat16),
            jax.ShapeDtypeStruct((length, out_cols), jnp.bfloat16),
            jax.ShapeDtypeStruct((ROPE, length), jnp.bfloat16),
            jax.ShapeDtypeStruct((1, out_cols), jnp.bfloat16),
        ),
        in_specs=[
            pl.BlockSpec((groups, 1, rows, part), lambda b: (0, b, 0, 0)),
            whole((1, cols)),
            whole((cols, out_cols)),
            whole((cols, out_cols)),
            whole(q_nope.shape),
            whole(q_rope.shape),
            pl.BlockSpec((1, rows, LANES), lambda b: (b, 0, 0)),
        ],
        out_specs=(
            pl.BlockSpec((rows, out_cols), lambda b: (b, 0)),
            pl.BlockSpec((rows, out_cols), lambda b: (b, 0)),
            pl.BlockSpec((ROPE, rows), lambda b: (0, b)),
            whole((1, out_cols)),
        ),
        scratch_shapes=[
            pltpu.VMEM((n_blocks, heads, rows), jnp.float32),
            pltpu.VMEM((n_blocks, rows, out_cols), jnp.bfloat16),
        ],
    )(latent, kv_gain, w_up_key, w_up_value, q_nope, q_rope, rope)


def local(
    tokens, offsets, in_gain, w_latent, w_rope_key, kv_gain, w_up_key, w_up_value, q_nope, q_rope
):
    frequency = np.float32(10000.0) ** (-np.arange(0, ROPE, 2).astype(np.float32) / ROPE)
    inverse = np.zeros((1, LANES), np.float32)
    inverse[0, :ROPE] = np.concatenate([frequency, frequency])
    inverse = jnp.asarray(inverse)
    latent, rope = gather_latent(tokens, w_latent, w_rope_key.T, in_gain[None], offsets, inverse)
    keys, values, rope_keys, read = fill_cache(
        latent, kv_gain[None], w_up_key, w_up_value, q_nope, q_rope, rope
    )
    return (keys[None], values[None], rope_keys[None], read)


def solution(mesh):
    in_specs = (
        P(("grp", "tp"), "sp", None),
        P(("grp", "tp")),
        P(),
        P("sp", None),
        P(),
        P(),
        P(None, "tp"),
        P(None, "tp"),
        P(("grp", "sp"), "tp"),
        P(("grp", "sp"), "tp"),
    )
    out_specs = (
        P(("grp", "sp"), None, "tp"),
        P(("grp", "sp"), None, "tp"),
        P(("grp", "sp"), None, None),
        P(("grp", "sp"), "tp"),
    )
    return jax.shard_map(local, mesh=mesh, in_specs=in_specs, out_specs=out_specs, check_vma=False)
```

profile of v0, /device:TPU:1, one launch (start us, length us, event | category | flops | bytes accessed | tf_op | source)
XLA Modules:
  0.0 75.5 jit_solution(15425152097355622238)
XLA Ops:
  1.3 67.3 %shard_map.138 = (bf16[4,4,256,256]{3,2,1,0:T(8,128)(2,1)}, bf16[4,256,128]{2,1,0:T(8,128)(2,1)}) custom-call(bf16[256,4096]{1,0:T(8,128)(2,1)} %bitcast.7, bf16[1024,1024]{1,0:T(8,128)(2,1)} %w_hbm.1, bf16[32,4096]{1,0:T(8,128)(2,1)} %bitcast.8, f32[1,4096]{1,0:T(1,128)} %bitcast.9, s32[1]{0:T(128)S(6)} %copy.15.offsets, f32[1,128]{1,0:T(1,128)} %constant.2.clone.inverse), custom_call_target="tpu_custom_call" | custom-call | tf_op jit(solution)/shard_map/pallas_call | solution.py:425
  68.6 6.9 %shard_map.139 = (bf16[1024,512]{1,0:T(8,128)(2,1)}, bf16[1024,512]{1,0:T(8,128)(2,1)}, bf16[32,1024]{1,0:T(8,128)(2,1)}, bf16[1,512]{1,0:T(2,128)(2,1)}) custom-call(bf16[4,4,256,256]{3,2,1,0:T(8,128)(2,1)} %get-tuple-element.10.latent_ref, f32[1,1024]{1,0:T(1,128)} %bitcast.10, bf16[1024,512]{1,0:T(8,128)(2,1)} %wk_ref.1, bf16[1024,512]{1,0:T(8,128)(2,1)} %wv_ref.1, ...), custom_call_target="tpu_custom_call" | custom-call | tf_op jit(solution)/shard_map/pallas_call | solution.py:540
where the time goes:
time: 75.8 us; the launch traced here: 75.5 us
  Pallas kernels  74.2 us (98%)
  between operations  1.28 us (2%)
    pallas_call x1, Pallas kernels, gather_latent(): pl.pallas_call(functools.partial(gather_kernel, n_grp, n_sp, n_tp, groups...  67.3 us
    pallas_call x1, Pallas kernels, fill_cache(): pl.pallas_call(functools.partial(cache_kernel, n_blocks), grid=(n_blocks,...  6.9 us

commit v1 on v0

v1 whole, which is shorter than its diff:
```python
import functools

import jax
import jax.numpy as jnp
import numpy as np
from jax import lax
from jax.experimental import pallas as pl
from jax.experimental.pallas import tpu as pltpu
from jax.sharding import PartitionSpec as P

HEAD = 64
ROPE = 32
CORES = 2
PIECES = 4
PENDING = 60
PARTS = (1, 1, 1, 1, 1, 1, 1, 1)
MODES = ("F", "O", "F", "O", "F", "O", "C", "O", "F")
X_FIRST = (True, True, True, True, False, True, False, True, True, True, True, True, True, True, False, True, True, True, True, False, True, True, True, True)
OUTER = (
    ("own", 0), ("own", 1), ("own", 2), ("norm", 1), ("norm", 0), ("a", 0), ("norm", 2), ("a", 3),
    ("own", 3), ("norm", 3), ("odot", 0), ("odot", 5), ("b", 0), ("odot", 3), ("odot", 2),
    ("odot", 4), ("a", 1), ("odot", 6), ("odot", 7), ("own", 4), ("odot", 1), ("a", 9), ("b", 3),
    ("a", 6), ("a", 4), ("b", 1), ("a", 7), ("own", 5), ("a", 2), ("l", 0), ("b", 9), ("c", 3),
    ("b", 6), ("t", 0), ("b", 7), ("a", 10), ("a", 12), ("b", 4), ("c", 0), ("dot", 0), ("b", 2),
    ("c", 9), ("own", 6), ("c", 6), ("a", 5), ("a", 8), ("b", 10), ("c", 1), ("a", 11), ("dot", 6),
    ("d", 0, 0), ("d", 0, 2), ("d", 0, 3), ("d", 0, 1), ("a", 15), ("b", 12), ("dot", 3), ("c", 7),
    ("c", 4), ("dot", 1), ("a", 18), ("b", 8), ("a", 13), ("c", 2), ("a", 16), ("own", 7),
    ("dot", 7), ("dot", 4), ("a", 14), ("b", 5), ("b", 16), ("b", 13), ("b", 11), ("b", 15),
    ("dot", 2), ("l", 1), ("a", 17), ("a", 21), ("c", 12), ("a", 19), ("c", 10), ("b", 18),
    ("a", 20), ("dot", 10), ("b", 21), ("d", 1, 2), ("dot", 12), ("a", 22), ("b", 20), ("c", 8),
    ("c", 13), ("b", 17), ("c", 5), ("b", 14), ("dot", 9), ("a", 23), ("dot", 8), ("l", 3),
    ("dot", 5), ("l", 2), ("c", 11), ("b", 22), ("b", 23), ("c", 14), ("c", 15), ("d", 1, 3),
    ("dot", 13), ("dot", 11), ("l", 4), ("b", 19), ("d", 1, 1), ("t", 2), ("d", 1, 0), ("dot", 14),
    ("l", 5), ("d", 5, 1), ("dot", 15), ("c", 16), ("d", 2, 0), ("c", 18), ("d", 2, 2), ("c", 17),
    ("t", 4), ("e", 1, 3), ("dot", 18), ("c", 20), ("c", 19), ("dot", 16), ("e", 1, 2), ("d", 2, 3),
    ("d", 2, 1), ("dot", 19), ("d", 3, 2), ("dot", 17), ("l", 6), ("c", 21), ("d", 4, 2),
    ("d", 4, 1), ("dot", 21), ("d", 4, 0), ("e", 1, 1), ("dot", 20), ("l", 7), ("d", 3, 1),
    ("d", 5, 3), ("d", 3, 3), ("d", 4, 3), ("d", 5, 2), ("t", 6), ("c", 22), ("c", 23), ("d", 6, 2),
    ("dot", 22), ("d", 3, 0), ("dot", 23), ("l", 8), ("d", 6, 0), ("e", 5, 1), ("d", 7, 1),
    ("e", 3, 1), ("d", 6, 3), ("d", 6, 1), ("d", 7, 2), ("e", 5, 2), ("e", 5, 3), ("e", 3, 2),
    ("e", 6, 2), ("d", 7, 0), ("d", 7, 3), ("e", 7, 1), ("t", 8), ("e", 6, 1), ("e", 6, 3),
    ("d", 8, 1), ("d", 5, 0), ("e", 3, 3), ("e", 7, 2), ("e", 7, 3), ("d", 8, 0), ("d", 8, 2),
    ("d", 8, 3), ("end", 0, 0), ("end", 0, 1), ("end", 0, 2), ("end", 0, 3), ("end", 1, 0),
    ("end", 1, 1), ("end", 1, 2), ("end", 1, 3), ("end", 2, 0), ("end", 2, 1), ("end", 2, 2),
    ("end", 2, 3), ("end", 3, 0), ("end", 3, 1), ("end", 3, 2), ("end", 3, 3), ("end", 4, 0),
    ("end", 4, 1), ("end", 4, 2), ("end", 4, 3), ("end", 5, 0), ("end", 5, 1), ("end", 5, 2),
    ("end", 5, 3), ("end", 6, 0), ("end", 6, 1), ("end", 6, 2), ("end", 6, 3), ("end", 7, 0),
    ("end", 7, 1), ("end", 7, 2), ("end", 7, 3), ("end", 8, 0), ("end", 8, 1), ("end", 8, 2),
    ("end", 8, 3),
)
MIDDLE = (
    ("own", 0), ("own", 1), ("norm", 1), ("own", 2), ("norm", 0), ("norm", 2), ("z", 0), ("a", 0),
    ("z", 1), ("a", 1), ("own", 3), ("z", 4), ("a", 4), ("norm", 3), ("odot", 1), ("odot", 3),
    ("z", 7), ("a", 7), ("odot", 2), ("odot", 4), ("z", 2), ("a", 2), ("odot", 6), ("b", 1),
    ("z", 6), ("a", 6), ("z", 3), ("z", 9), ("a", 9), ("a", 3), ("odot", 0), ("z", 10), ("b", 4),
    ("odot", 7), ("l", 0), ("own", 4), ("a", 10), ("b", 0), ("c", 1), ("z", 5), ("a", 5), ("z", 8),
    ("a", 8), ("b", 7), ("b", 6), ("b", 3), ("z", 12), ("a", 12), ("z", 13), ("own", 5), ("t", 0),
    ("a", 13), ("z", 11), ("a", 11), ("b", 9), ("b", 2), ("odot", 5), ("z", 15), ("a", 15),
    ("c", 4), ("c", 0), ("dot", 0), ("c", 7), ("d", 0, 1), ("b", 10), ("z", 16), ("a", 16),
    ("dot", 1), ("own", 6), ("z", 14), ("a", 14), ("c", 6), ("b", 5), ("b", 8), ("z", 17),
    ("dot", 4), ("z", 19), ("own", 7), ("b", 12), ("c", 3), ("c", 2), ("d", 0, 0), ("b", 11),
    ("d", 0, 2), ("z", 18), ("a", 18), ("dot", 3), ("b", 13), ("a", 17), ("a", 19), ("dot", 6),
    ("c", 9), ("dot", 2), ("l", 1), ("b", 14), ("c", 10), ("b", 16), ("z", 21), ("a", 21),
    ("b", 15), ("z", 20), ("a", 20), ("b", 17), ("z", 22), ("a", 22), ("c", 5), ("c", 8), ("z", 23),
    ("a", 23), ("b", 18), ("dot", 7), ("dot", 5), ("l", 2), ("dot", 8), ("l", 3), ("d", 0, 3),
    ("c", 11), ("d", 1, 2), ("b", 20), ("dot", 9), ("c", 14), ("dot", 10), ("b", 19), ("dot", 14),
    ("b", 22), ("c", 12), ("d", 1, 1), ("d", 1, 0), ("dot", 11), ("l", 4), ("c", 13), ("b", 23),
    ("d", 1, 3), ("b", 21), ("dot", 13), ("d", 3, 2), ("dot", 12), ("l", 5), ("t", 2), ("c", 19),
    ("c", 16), ("c", 15), ("dot", 15), ("t", 4), ("d", 4, 0), ("c", 17), ("dot", 17), ("d", 3, 1),
    ("d", 3, 0), ("c", 18), ("dot", 19), ("e", 1, 2), ("d", 5, 2), ("d", 3, 3), ("c", 20),
    ("d", 2, 0), ("dot", 16), ("l", 6), ("d", 4, 2), ("dot", 18), ("e", 3, 1), ("d", 5, 0),
    ("e", 1, 1), ("t", 6), ("dot", 20), ("l", 7), ("d", 4, 1), ("c", 22), ("dot", 22), ("d", 4, 3),
    ("c", 21), ("c", 23), ("d", 5, 1), ("dot", 21), ("d", 2, 2), ("d", 5, 3), ("dot", 23), ("l", 8),
    ("d", 7, 2), ("e", 1, 3), ("d", 2, 1), ("e", 3, 2), ("d", 2, 3), ("d", 6, 2), ("d", 7, 1),
    ("d", 7, 3), ("t", 8), ("e", 5, 1), ("e", 5, 3), ("d", 6, 1), ("e", 3, 3), ("e", 5, 2),
    ("d", 6, 0), ("d", 7, 0), ("e", 7, 2), ("d", 6, 3), ("e", 6, 1), ("e", 6, 2), ("e", 7, 3),
    ("e", 6, 3), ("d", 8, 1), ("d", 8, 0), ("e", 7, 1), ("d", 8, 3), ("d", 8, 2), ("end", 0, 0),
    ("end", 0, 1), ("end", 0, 2), ("end", 0, 3), ("end", 1, 0), ("end", 1, 1), ("end", 1, 2),
    ("end", 1, 3), ("end", 2, 0), ("end", 2, 1), ("end", 2, 2), ("end", 2, 3), ("end", 3, 0),
    ("end", 3, 1), ("end", 3, 2), ("end", 3, 3), ("end", 4, 0), ("end", 4, 1), ("end", 4, 2),
    ("end", 4, 3), ("end", 5, 0), ("end", 5, 1), ("end", 5, 2), ("end", 5, 3), ("end", 6, 0),
    ("end", 6, 1), ("end", 6, 2), ("end", 6, 3), ("end", 7, 0), ("end", 7, 1), ("end", 7, 2),
    ("end", 7, 3), ("end", 8, 0), ("end", 8, 1), ("end", 8, 2), ("end", 8, 3),
)

EPS = 1e-06
MESH = pl.DeviceIdType.MESH


def column_groups(n_sp, cols):
    if n_sp > 4 or cols % 1024:
        return [(0, cols)]
    each, total, out = cols // sum(PARTS), 0, []
    for part in PARTS:
        out.append((total, part * each))
        total += part * each
    return out


def plain_schedule(units, groups, n_sp):
    late = len(units) * 10
    ops = [(g, ("own", g)) for g in range(groups)]
    ops += [(k, ("norm", k)) for k in range(PIECES)]
    ops += [(PIECES + g, ("odot", g)) for g in range(groups)]
    done = {}
    for u, (g, d) in enumerate(units):
        at = PIECES + 2 + u
        ops += [(at, ("a", u)), (at + 2, ("b", u)), (at + 4, ("c", u)), (at + 5, ("dot", u))]
        done[g + 1] = at + 5
    for m in range(groups + 1):
        at = done.get(m, PIECES + 1)
        ops += [(at + 0.5, ("l", m)), (at + 3, ("t", m))]
        ops += [(at + 6, ("d", m, d)) for d in range(n_sp)]
        ops += [(late + m, ("end", m, d)) for d in range(n_sp)]
    return [op for _, op in sorted(ops, key=lambda item: item[0])]


def gather_kernel(n_grp, n_sp, n_tp, spans, frequency, *refs):
    groups = len(spans)
    tok_hbm, w_hbm, w_rope_hbm, gain_hbm, offsets, lat_out, rope_out = refs[:7]
    tok, w_own, w_rope, in_gain, normed = refs[7:12]
    wbuf, acc, own, transit = (refs[12 + k * groups : 12 + (k + 1) * groups] for k in range(4))
    (
        own_rope,
        transit_rope,
        local_sem,
        own_send,
        z_send,
        z_recv,
        a_send,
        a_recv,
        b_send,
        b_recv,
        c_send,
        c_recv,
        l_send,
        t_send,
        t_recv,
        x_send,
        e_send,
        d_send,
        l_recv,
    ) = refs[12 + 4 * groups :]
    n_x = n_tp // CORES
    prompts, rows = own[0].shape[:2]
    depth, cols = w_own.shape
    chunk = depth // (n_grp * n_tp)
    y, z, t = lax.axis_index("grp"), lax.axis_index("sp"), lax.axis_index("tp")
    x, core = t // CORES, t % CORES
    rank = (core * n_x + x) * n_grp + y

    def tp_of(x_to, core_to):
        return {"tp": x_to * CORES + core_to}

    partner = tp_of(x, 1 - core)
    x_peers = [lax.rem(x + k, n_x) for k in range(1, n_x)]
    y_peers = [lax.rem(y + k, n_grp) for k in range(1, n_grp)]
    z_up, z_down = lax.rem(z + 1, n_sp), lax.rem(z + n_sp - 1, n_sp)
    has_up, has_down = z + 1 < n_sp, z > 0

    fetch_tok = pltpu.make_async_copy(tok_hbm, tok, local_sem.at[0])
    fetch_w = pltpu.make_async_copy(w_hbm, w_own, local_sem.at[1])
    fetch_rope = pltpu.make_async_copy(w_rope_hbm, w_rope, local_sem.at[2])
    fetch_gain = pltpu.make_async_copy(gain_hbm, in_gain, local_sem.at[3])

    barrier = pltpu.get_barrier_semaphore()

    def greet(target):
        pl.semaphore_signal(barrier, inc=1, device_id=target, device_id_type=MESH)

    pl.when(has_up)(lambda: greet({"sp": z_up}))
    pl.when(has_down)(lambda: greet({"sp": z_down}))
    near = [tp_of(p, core) for p in x_peers] + [{"grp": p} for p in y_peers] + [partner]
    for target in near:
        greet(target)
    fetch_gain.start()
    fetch_tok.start()
    fetch_w.start()
    fetch_rope.start()
    pl.semaphore_wait(barrier, len(near) + has_up.astype(jnp.int32) + has_down.astype(jnp.int32))

    finish, fetched = [], []
    tuned = n_sp == 4 and groups == len(PARTS)
    modes = MODES if tuned else ("F",) * (groups + 1)

    def remote(src, dst, send, recv, device):
        return pltpu.make_async_remote_copy(
            src_ref=src,
            dst_ref=dst,
            send_sem=send,
            recv_sem=recv,
            device_id=device,
            device_id_type=MESH,
        )

    def arrived(ref, recv):
        remote(ref, ref, recv, recv, partner).wait_recv()

    def need(copy):
        if not any(copy is other for other in fetched):
            fetched.append(copy)
            copy.wait()

    def begin(copy, when=None):
        if when is None:
            copy.start()
            finish.append(copy.wait_send)
        else:
            pl.when(when)(copy.start)
            finish.append(lambda: pl.when(when)(copy.wait_send))

    units = [(g, d) for g in range(groups) for d in range(1, n_sp)]
    above = n_sp - 1 - z
    both = jnp.minimum(z, above)

    def shard(d):
        paired = d <= 2 * both
        hop = jnp.where(paired, (d + 1) // 2, d - both)
        up = jnp.where(paired, d % 2 == 1, above > z)
        return jnp.where(up, z + hop, z - hop), up

    shards = {d: shard(d) for d in range(1, n_sp)}

    def own_z(g):
        first, width = spans[g]
        for side, ahead, exists in ((0, z_up, has_up), (1, z_down, has_down)):
            copy = remote(
                w_hbm.at[pl.ds(rank * chunk, chunk), pl.ds(first, width)],
                wbuf[g].at[z, core, x, y],
                own_send.at[g, side],
                z_recv.at[g, z],
                {"sp": ahead},
            )
            begin(copy, exists)

    def x_first(u):
        return X_FIRST[u] if tuned else u % 4 > 0

    def spread(u, src, send, recv, along_x):
        peers = x_peers if along_x else y_peers
        for k, peer in enumerate(peers):
            device = tp_of(peer, core) if along_x else {"grp": peer}
            begin(remote(src, src, send.at[u, k], recv.at[u, k], device))

    def block_a(u):
        g, d = units[u]
        return wbuf[g].at[shards[d][0], core, x, y]

    def block_b(u):
        g, d = units[u]
        if x_first(u):
            return wbuf[g].at[shards[d][0], core, :, y]
        return wbuf[g].at[shards[d][0], core, x]

    def stage_z(u):
        g, d = units[u]
        s, up = shards[d]
        arrived(block_a(u), z_recv.at[g, s])
        exists = jnp.where(up, has_down, has_up)
        ahead = jnp.where(up, z_down, z_up)
        begin(
            remote(block_a(u), block_a(u), z_send.at[u], z_recv.at[g, s], {"sp": ahead}), exists
        )

    def stage_a(u):
        spread(u, block_a(u), a_send, a_recv, x_first(u))

    def stage_b(u):
        for k in range(len(x_peers if x_first(u) else y_peers)):
            arrived(block_a(u), a_recv.at[u, k])
        spread(u, block_b(u), b_send, b_recv, not x_first(u))

    def stage_c(u):
        g, d = units[u]
        for k in range(len(y_peers if x_first(u) else x_peers)):
            arrived(block_b(u), b_recv.at[u, k])
        ref = wbuf[g].at[shards[d][0], core]
        begin(remote(ref, ref, c_send.at[u], c_recv.at[u], partner))

    def stage_dot(u):
        g, d = units[u]
        s, _ = shards[d]
        arrived(wbuf[g].at[s, core], c_recv.at[u])
        weight = wbuf[g][s].reshape(depth, spans[g][1])
        acc[g][...] += jnp.dot(normed[s], weight, preferred_element_type=jnp.float32)

    def slot(m, s):
        if m == 0:
            return rope_out.at[s]
        first, width = spans[m - 1]
        return lat_out.at[s, :, pl.ds(first, width)]

    def mine(m, i):
        return own_rope.at[i] if m == 0 else own[m - 1].at[i]

    def held(m, k, i):
        return transit_rope.at[k, i] if m == 0 else transit[m - 1].at[k, i]

    def stage_l(m):
        for i in range(prompts):
            home = t * prompts + i
            if modes[m] != "C":
                copy = remote(
                    mine(m, i), slot(m, z), l_send.at[m, i], l_recv.at[m, z], {"sp": home}
                )
                begin(copy, home != z)
            for k, peer in enumerate(x_peers):
                device = tp_of(peer, core)
                beside = remote(mine(m, i), slot(m, z), x_send.at[m, i, k], l_recv.at[m, z], device)
                begin(beside, home == z)
                if modes[m] == "D":
                    routed = remote(
                        mine(m, i),
                        slot(m, z),
                        x_send.at[m, i, k],
                        l_recv.at[m, z],
                        device | {"sp": home},
                    )
                    begin(routed, home != z)
                elif modes[m] != "O":
                    across = remote(
                        mine(m, i), held(m, k, i), x_send.at[m, i, k], t_recv.at[m, k, i], device
                    )
                    begin(across, home != z)

    def stage_t(m):
        if modes[m] not in "FC":
            return
        for k in range(n_x - 1):
            source = lax.rem(x + n_x - 1 - k, n_x) * CORES + core
            for i in range(prompts):
                home = source * prompts + i
                copy = remote(
                    held(m, k, i), slot(m, z), t_send.at[m, k, i], l_recv.at[m, z], {"sp": home}
                )

                def pass_on(k=k, i=i, copy=copy):
                    arrived(held(m, k, i), t_recv.at[m, k, i])
                    copy.start()

                pl.when(home != z)(pass_on)
                finish.append(lambda home=home, copy=copy: pl.when(home != z)(copy.wait_send))

    owner = z // prompts
    x_in, core_in = owner // CORES, owner % CORES

    def partner_copy(m, d, s):
        return remote(slot(m, s), slot(m, s), d_send.at[m, d], l_recv.at[m, s], partner)

    def enters(m, d):
        here = core == core_in
        if d == 0 or modes[m] in "FD":
            return here
        return here & ((x == x_in) if modes[m] == "O" else (x != x_in))

    def stage_d(m, d):
        s = z if d == 0 else shards[d][0]
        copies = [partner_copy(m, d, s)]
        if d and modes[m] in "OC":
            copies += [
                remote(slot(m, s), slot(m, s), e_send.at[m, d, k], l_recv.at[m, s], tp_of(peer, core))
                for k, peer in enumerate(x_peers)
            ]

        def hand():
            if d == 0:
                pl.when(x != x_in)(lambda: arrived(slot(m, s), l_recv.at[m, s]))
            else:
                arrived(slot(m, s), l_recv.at[m, s])
            for copy in reversed(copies):
                copy.start()

        def drain():
            for copy in copies:
                copy.wait_send()

        pl.when(enters(m, d))(hand)
        finish.append(lambda: pl.when(enters(m, d))(drain))

    def stage_e(m, d):
        s = shards[d][0]
        here = (core == core_in) & jnp.logical_not(enters(m, d))
        copy = partner_copy(m, d, s)

        def hand():
            arrived(slot(m, s), l_recv.at[m, s])
            copy.start()

        pl.when(here)(hand)
        finish.append(lambda: pl.when(here)(copy.wait_send))

    def stage_end(m, d):
        s = z if d == 0 else shards[d][0]
        pl.when(core != core_in)(lambda: arrived(slot(m, s), l_recv.at[m, s]))

    def finalize(m, values):
        for i in range(prompts):
            mine(m, i)[...] = values[i]

            def keep(i=i):
                slot(m, z)[...] = values[i]

            pl.when(t * prompts + i == z)(keep)

    step_rows, pieces = 16, PIECES

    def norm(r, carry):
        at = pl.ds(pl.multiple_of(r * step_rows, step_rows), step_rows)
        wide = tok[at, :].astype(jnp.float32)
        scale = lax.rsqrt(jnp.mean(wide * wide, axis=-1, keepdims=True) + EPS)
        out = (wide * scale * in_gain[...]).astype(jnp.bfloat16)
        for b in range(n_sp):
            normed[b, at, :] = out[:, b * depth : (b + 1) * depth]
        return carry

    def norm_piece(k):
        need(fetch_gain)
        need(fetch_tok)
        turns = prompts * rows // step_rows // pieces
        lax.fori_loop(k * turns, (k + 1) * turns, norm, 0)

    def own_dot(g):
        first, width = spans[g]
        need(fetch_w)
        acc[g][...] = jnp.dot(
            normed[z], w_own[:, first : first + width], preferred_element_type=jnp.float32
        )

    def rope_item():
        need(fetch_rope)
        raw = jnp.zeros((ROPE, prompts * rows), jnp.float32)
        for b in range(n_sp):
            raw += lax.dot_general(
                w_rope[:, b * depth : (b + 1) * depth],
                normed[b],
                (((1,), (1,)), ((), ())),
                preferred_element_type=jnp.float32,
            )
        half = ROPE // 2
        index = lax.broadcasted_iota(jnp.int32, (half, rows), 1)
        channel = lax.broadcasted_iota(jnp.int32, (half, rows), 0)
        inverse = jnp.zeros((half, rows), jnp.float32)
        for c, value in enumerate(frequency):
            inverse = jnp.where(channel == c, value, inverse)
        values = []
        for i in range(prompts):
            position = offsets[i] + z * rows + index
            angle = position.astype(jnp.float32) * inverse
            sine, cosine = jnp.sin(angle), jnp.cos(angle)
            first = raw[:half, i * rows : (i + 1) * rows]
            second = raw[half:, i * rows : (i + 1) * rows]
            turned = [first * cosine - second * sine, second * cosine + first * sine]
            values.append(jnp.concatenate(turned, axis=0).astype(jnp.bfloat16))
        finalize(0, values)

    def group_item(g):
        value = acc[g][...].astype(jnp.bfloat16)
        finalize(g + 1, [value[i * rows : (i + 1) * rows] for i in range(prompts)])

    def latent_item(m):
        if m == 0:
            rope_item()
        else:
            group_item(m - 1)
        stage_l(m)

    stages = {
        "own": own_z,
        "norm": norm_piece,
        "odot": own_dot,
        "z": stage_z,
        "a": stage_a,
        "b": stage_b,
        "c": stage_c,
        "dot": stage_dot,
        "l": latent_item,
        "t": stage_t,
        "d": stage_d,
        "e": stage_e,
        "end": stage_end,
    }

    def run(schedule, middle):
        finish.clear()
        fetched.clear()
        for name, *args in schedule:
            if name == "a" and not middle:
                stage_z(*args)
            stages[name](*args)
            while len(finish) > PENDING:
                finish.pop(0)()
        for fn in finish:
            fn()

    if tuned:
        inner = has_up & has_down
        pl.when(inner)(lambda: run(MIDDLE, True))
        pl.when(jnp.logical_not(inner))(lambda: run(OUTER, False))
    else:
        run(plain_schedule(units, groups, n_sp), False)


def gather_latent(tokens, w_latent, w_rope, in_gain, offsets, frequency):
    prompts, rows, width = tokens.shape
    n_grp, n_sp, n_tp = (lax.axis_size(a) for a in ("grp", "sp", "tp"))
    n_x = n_tp // CORES
    depth, cols = w_latent.shape
    spans = column_groups(n_sp, cols)
    groups = len(spans)
    chunk = depth // (n_grp * n_tp)
    total = prompts * rows
    units = groups * (n_sp - 1)
    peers = max(n_x, n_grp) - 1
    others = max(n_x - 1, 1)
    items = groups + 1
    bf16, f32 = jnp.bfloat16, jnp.float32
    dma = pltpu.SemaphoreType.DMA
    stay = lambda a: pltpu.with_memory_space_constraint(a, pltpu.HBM)
    limit = (40 if groups > 1 else 60) * 1024 * 1024
    vmem = pl.BlockSpec(memory_space=pltpu.VMEM)
    hbm = pl.BlockSpec(memory_space=pltpu.HBM)
    return pl.pallas_call(
        functools.partial(gather_kernel, n_grp, n_sp, n_tp, spans, frequency),
        out_shape=(
            jax.ShapeDtypeStruct((n_sp, rows, cols), bf16),
            jax.ShapeDtypeStruct((n_sp, ROPE, rows), bf16),
        ),
        in_specs=[hbm, hbm, hbm, hbm, pl.BlockSpec(memory_space=pltpu.SMEM)],
        out_specs=(vmem, vmem),
        scratch_shapes=[
            pltpu.VMEM((total, width), bf16),
            pltpu.VMEM((depth, cols), bf16),
            pltpu.VMEM((ROPE, width), bf16),
            pltpu.VMEM((1, width), f32),
            pltpu.VMEM((n_sp, total, depth), bf16),
            *[pltpu.VMEM((n_sp, CORES, n_x, n_grp, chunk, w), bf16) for _, w in spans],
            *[pltpu.VMEM((total, w), f32) for _, w in spans],
            *[pltpu.VMEM((prompts, rows, w), bf16) for _, w in spans],
            *[pltpu.VMEM((others, prompts, rows, w), bf16) for _, w in spans],
            pltpu.VMEM((prompts, ROPE, rows), bf16),
            pltpu.VMEM((others, prompts, ROPE, rows), bf16),
            dma((4,)),
            dma((groups, 2)),
            dma((units,)),
            dma((groups, n_sp)),
            dma((units, peers)),
            dma((units, peers)),
            dma((units, peers)),
            dma((units, peers)),
            dma((units,)),
            dma((units,)),
            dma((items, prompts)),
            dma((items, others, prompts)),
            dma((items, others, prompts)),
            dma((items, prompts, others)),
            dma((items, n_sp, others)),
            dma((items, n_sp)),
            dma((items, n_sp)),
        ],
        compiler_params=pltpu.CompilerParams(
            collective_id=0, has_side_effects=True, vmem_limit_bytes=limit
        ),
    )(*map(stay, (tokens.reshape(total, width), w_latent, w_rope, in_gain)), offsets)


def cache_kernel(
    n_blocks,
    latent_ref,
    gain_ref,
    wk_ref,
    wv_ref,
    q_nope_ref,
    q_rope_ref,
    rope_ref,
    keys_ref,
    values_ref,
    rope_keys_ref,
    read_ref,
    scores,
    held,
):
    b = pl.program_id(0)
    heads = scores.shape[1]

    def per_head(row, size):
        wide = jnp.broadcast_to(row.astype(jnp.float32), (heads, heads * size))
        head = lax.broadcasted_iota(jnp.int32, wide.shape, 0)
        lane = lax.broadcasted_iota(jnp.int32, wide.shape, 1)
        return jnp.where((lane >= head * size) & (lane < head * size + size), wide, 0.0)

    query = per_head(q_nope_ref[...], HEAD).astype(jnp.bfloat16)
    spread = (heads * ROPE, ROPE)
    fold = lax.broadcasted_iota(jnp.int32, spread, 0) % ROPE == lax.broadcasted_iota(
        jnp.int32, spread, 1
    )
    rotary_q = jnp.dot(
        per_head(q_rope_ref[...], ROPE).astype(jnp.bfloat16),
        jnp.where(fold, 1.0, 0.0).astype(jnp.bfloat16),
        preferred_element_type=jnp.float32,
    ).astype(jnp.bfloat16)
    raw = latent_ref[0].astype(jnp.float32)
    scale = lax.rsqrt(jnp.mean(raw * raw, axis=-1, keepdims=True) + EPS)
    latent = (raw * scale * gain_ref[...]).astype(jnp.bfloat16)
    keys = jnp.dot(latent, wk_ref[...], preferred_element_type=jnp.float32).astype(jnp.bfloat16)
    keys_ref[...] = keys
    values = jnp.dot(latent, wv_ref[...], preferred_element_type=jnp.float32).astype(jnp.bfloat16)
    values_ref[...] = values
    held[b] = values
    rope = rope_ref[0]
    rope_keys_ref[...] = rope
    across = (((1,), (1,)), ((), ()))
    part = lax.dot_general(query, keys, across, preferred_element_type=jnp.float32)
    part += jnp.dot(rotary_q, rope, preferred_element_type=jnp.float32)
    scores[b] = part / jnp.sqrt(jnp.float32(HEAD + ROPE))

    @pl.when(b == n_blocks - 1)
    def _():
        every = scores[...]
        peak = jnp.max(jnp.max(every, axis=-1, keepdims=True), axis=0, keepdims=True)
        expo = jnp.exp(every - peak)
        total = jnp.sum(jnp.sum(expo, axis=-1, keepdims=True), axis=0, keepdims=True)
        weights = (expo / total).astype(jnp.bfloat16)
        out = jnp.dot(weights[0], held[0], preferred_element_type=jnp.float32)
        for i in range(1, n_blocks):
            out += jnp.dot(weights[i], held[i], preferred_element_type=jnp.float32)
        head = lax.broadcasted_iota(jnp.int32, out.shape, 0)
        lane = lax.broadcasted_iota(jnp.int32, out.shape, 1)
        picked = jnp.where((lane >= head * HEAD) & (lane < head * HEAD + HEAD), out, 0.0)
        read_ref[...] = jnp.sum(picked, axis=0, keepdims=True).astype(jnp.bfloat16)


def fill_cache(latent, kv_gain, w_up_key, w_up_value, q_nope, q_rope, rope):
    n_blocks, rows, cols = latent.shape
    out_cols = w_up_key.shape[1]
    heads = out_cols // HEAD
    length = n_blocks * rows
    whole = lambda shape: pl.BlockSpec(shape, lambda b: (0,) * len(shape))
    return pl.pallas_call(
        functools.partial(cache_kernel, n_blocks),
        grid=(n_blocks,),
        out_shape=(
            jax.ShapeDtypeStruct((length, out_cols), jnp.bfloat16),
            jax.ShapeDtypeStruct((length, out_cols), jnp.bfloat16),
            jax.ShapeDtypeStruct((ROPE, length), jnp.bfloat16),
            jax.ShapeDtypeStruct((1, out_cols), jnp.bfloat16),
        ),
        in_specs=[
            pl.BlockSpec((1, rows, cols), lambda b: (b, 0, 0)),
            whole((1, cols)),
            whole((cols, out_cols)),
            whole((cols, out_cols)),
            whole(q_nope.shape),
            whole(q_rope.shape),
            pl.BlockSpec((1, ROPE, rows), lambda b: (b, 0, 0)),
        ],
        out_specs=(
            pl.BlockSpec((rows, out_cols), lambda b: (b, 0)),
            pl.BlockSpec((rows, out_cols), lambda b: (b, 0)),
            pl.BlockSpec((ROPE, rows), lambda b: (0, b)),
            whole((1, out_cols)),
        ),
        scratch_shapes=[
            pltpu.VMEM((n_blocks, heads, rows), jnp.float32),
            pltpu.VMEM((n_blocks, rows, out_cols), jnp.bfloat16),
        ],
        compiler_params=pltpu.CompilerParams(vmem_limit_bytes=30 * 1024 * 1024),
    )(latent, kv_gain, w_up_key, w_up_value, q_nope, q_rope, rope)


def local(
    tokens, offsets, in_gain, w_latent, w_rope_key, kv_gain, w_up_key, w_up_value, q_nope, q_rope
):
    steps = -np.arange(0, ROPE, 2).astype(np.float32) / ROPE
    frequency = [float(f) for f in np.float32(10000.0) ** steps]
    latent, rope = gather_latent(tokens, w_latent, w_rope_key.T, in_gain[None], offsets, frequency)
    keys, values, rope_keys, read = fill_cache(
        latent, kv_gain[None], w_up_key, w_up_value, q_nope, q_rope, rope
    )
    return (keys[None], values[None], rope_keys[None], read)


def solution(mesh):
    in_specs = (
        P(("grp", "tp"), "sp", None),
        P(("grp", "tp")),
        P(),
        P("sp", None),
        P(),
        P(),
        P(None, "tp"),
        P(None, "tp"),
        P(("grp", "sp"), "tp"),
        P(("grp", "sp"), "tp"),
    )
    out_specs = (
        P(("grp", "sp"), None, "tp"),
        P(("grp", "sp"), None, "tp"),
        P(("grp", "sp"), None, None),
        P(("grp", "sp"), "tp"),
    )
    return jax.shard_map(local, mesh=mesh, in_specs=in_specs, out_specs=out_specs, check_vma=False)
```

time: 75.8 us -> 68.8 us (0.908)
  Pallas kernels: 74.2 us -> 67.1 us
    pallas_call x1, Pallas kernels: 67.3 us -> 62.4 us  [gather_latent(): pl.pallas_call(functools.partial(gather_kernel, n_grp, n_sp, n_tp, spans,...]
    pallas_call x1, Pallas kernels: 6.9 us -> 4.77 us  [fill_cache(): pl.pallas_call(functools.partial(cache_kernel, n_blocks), grid=(n_blocks,...]
where the time goes in v1:
time: 68.8 us; the launch traced here: 68.7 us
  Pallas kernels  67.1 us (98%)
  between operations  1.51 us (2%)
    pallas_call x1, Pallas kernels, gather_latent(): pl.pallas_call(functools.partial(gather_kernel, n_grp, n_sp, n_tp, spans,...  62.4 us
    pallas_call x1, Pallas kernels, fill_cache(): pl.pallas_call(functools.partial(cache_kernel, n_blocks), grid=(n_blocks,...  4.77 us

profile of v1, /device:TPU:1, one launch (start us, length us, event | category | flops | bytes accessed | tf_op | source)
XLA Modules:
  0.0 68.7 jit_solution(12252834519250163281)
XLA Ops:
  1.3 0.0 copy-start
  1.3 0.0 copy-start.1
  1.3 0.0 copy-start.2
  1.3 0.0 copy-start.3
  1.3 0.0 copy-start.4
  1.3 62.4 %shard_map.129 = (bf16[4,256,1024]{2,1,0:T(8,128)(2,1)S(1)}, bf16[4,32,256]{2,1,0:T(8,128)(2,1)S(1)}) custom-call(bf16[256,4096]{1,0:T(8,128)(2,1)} %bitcast.8, bf16[1024,1024]{1,0:T(8,128)(2,1)} %refs_1_.1, bf16[32,4096]{1,0:T(8,128)(2,1)} %bitcast.9, f32[1,4096]{1,0:T(1,128)} %bitcast.10, s32[1]{0:T(128)S(6)} %copy.14.refs_4_), custom_call_target="tpu_custom_call" | custom-call | tf_op jit(solution)/shard_map/pallas_call | solution.py:522
  63.7 0.0 copy-done
  63.7 0.0 copy-done.1
  63.7 0.0 copy-done.2
  63.7 0.0 copy-done.3
  63.8 0.0 copy-done.4
  63.8 4.8 %shard_map.130 = (bf16[1024,512]{1,0:T(8,128)(2,1)}, bf16[1024,512]{1,0:T(8,128)(2,1)}, bf16[32,1024]{1,0:T(8,128)(2,1)}, bf16[1,512]{1,0:T(2,128)(2,1)}) custom-call(bf16[4,256,1024]{2,1,0:T(8,128)(2,1)S(1)} %get-tuple-element.10.latent_ref, f32[1,1024]{1,0:T(1,128)S(1)} %bitcast.7, bf16[1024,512]{1,0:T(8,128)(2,1)S(1)} %copy-done, ...), custom_call_target="tpu_custom_call" | custom-call | tf_op jit(solution)/shard_map/pallas_call | solution.py:638
Async XLA Ops:
  1.3 62.4 %copy-start = (bf16[1024,512]{1,0:T(8,128)(2,1)S(1)}, bf16[1024,512]{1,0:T(8,128)(2,1)}, u32[]{:S(2)}) copy-start(bf16[1024,512]{1,0:T(8,128)(2,1)} %wk_ref.1) | copy-start | bytes 3145732
  1.3 62.4 %copy-start.1 = (bf16[1024,512]{1,0:T(8,128)(2,1)S(1)}, bf16[1024,512]{1,0:T(8,128)(2,1)}, u32[]{:S(2)}) copy-start(bf16[1024,512]{1,0:T(8,128)(2,1)} %wv_ref.1) | copy-start | bytes 3145732
  1.3 62.4 %copy-start.2 = (f32[1024]{0:T(1024)S(1)}, f32[1024]{0:T(1024)}, u32[]{:S(2)}) copy-start(f32[1024]{0:T(1024)} %param.15) | copy-start | bytes 12292
  1.3 62.4 %copy-start.3 = (bf16[1,512]{1,0:T(2,128)(2,1)S(1)}, bf16[1,512]{1,0:T(2,128)(2,1)}, u32[]{:S(2)}) copy-start(bf16[1,512]{1,0:T(2,128)(2,1)} %q_nope_ref.1) | copy-start | bytes 3076
  1.3 62.4 %copy-start.4 = (bf16[1,256]{1,0:T(2,128)(2,1)S(1)}, bf16[1,256]{1,0:T(2,128)(2,1)}, u32[]{:S(2)}) copy-start(bf16[1,256]{1,0:T(2,128)(2,1)} %q_rope_ref.1) | copy-start | bytes 1540

commit v2 on v1

--- a/solution.py
+++ b/solution.py
@@ -14,33 +14,34 @@
 PIECES = 4
 PENDING = 60
 PARTS = (1, 1, 1, 1, 1, 1, 1, 1)
-MODES = ("F", "O", "F", "O", "F", "O", "C", "O", "F")
-X_FIRST = (True, True, True, True, False, True, False, True, True, True, True, True, True, True, False, True, True, True, True, False, True, True, True, True)
+MODES = ("F", "O", "F", "O", "C", "O", "C", "O", "O")
+X_FIRST = (True, False, False, False, True, True, True, False, True, True, True, True, False, True, True, False, True, True, False, False, True, True, True, False)
 OUTER = (
-    ("own", 0), ("own", 1), ("own", 2), ("norm", 1), ("norm", 0), ("a", 0), ("norm", 2), ("a", 3),
-    ("own", 3), ("norm", 3), ("odot", 0), ("odot", 5), ("b", 0), ("odot", 3), ("odot", 2),
-    ("odot", 4), ("a", 1), ("odot", 6), ("odot", 7), ("own", 4), ("odot", 1), ("a", 9), ("b", 3),
-    ("a", 6), ("a", 4), ("b", 1), ("a", 7), ("own", 5), ("a", 2), ("l", 0), ("b", 9), ("c", 3),
-    ("b", 6), ("t", 0), ("b", 7), ("a", 10), ("a", 12), ("b", 4), ("c", 0), ("dot", 0), ("b", 2),
-    ("c", 9), ("own", 6), ("c", 6), ("a", 5), ("a", 8), ("b", 10), ("c", 1), ("a", 11), ("dot", 6),
-    ("d", 0, 0), ("d", 0, 2), ("d", 0, 3), ("d", 0, 1), ("a", 15), ("b", 12), ("dot", 3), ("c", 7),
-    ("c", 4), ("dot", 1), ("a", 18), ("b", 8), ("a", 13), ("c", 2), ("a", 16), ("own", 7),
-    ("dot", 7), ("dot", 4), ("a", 14), ("b", 5), ("b", 16), ("b", 13), ("b", 11), ("b", 15),
-    ("dot", 2), ("l", 1), ("a", 17), ("a", 21), ("c", 12), ("a", 19), ("c", 10), ("b", 18),
-    ("a", 20), ("dot", 10), ("b", 21), ("d", 1, 2), ("dot", 12), ("a", 22), ("b", 20), ("c", 8),
-    ("c", 13), ("b", 17), ("c", 5), ("b", 14), ("dot", 9), ("a", 23), ("dot", 8), ("l", 3),
-    ("dot", 5), ("l", 2), ("c", 11), ("b", 22), ("b", 23), ("c", 14), ("c", 15), ("d", 1, 3),
-    ("dot", 13), ("dot", 11), ("l", 4), ("b", 19), ("d", 1, 1), ("t", 2), ("d", 1, 0), ("dot", 14),
-    ("l", 5), ("d", 5, 1), ("dot", 15), ("c", 16), ("d", 2, 0), ("c", 18), ("d", 2, 2), ("c", 17),
-    ("t", 4), ("e", 1, 3), ("dot", 18), ("c", 20), ("c", 19), ("dot", 16), ("e", 1, 2), ("d", 2, 3),
-    ("d", 2, 1), ("dot", 19), ("d", 3, 2), ("dot", 17), ("l", 6), ("c", 21), ("d", 4, 2),
-    ("d", 4, 1), ("dot", 21), ("d", 4, 0), ("e", 1, 1), ("dot", 20), ("l", 7), ("d", 3, 1),
-    ("d", 5, 3), ("d", 3, 3), ("d", 4, 3), ("d", 5, 2), ("t", 6), ("c", 22), ("c", 23), ("d", 6, 2),
-    ("dot", 22), ("d", 3, 0), ("dot", 23), ("l", 8), ("d", 6, 0), ("e", 5, 1), ("d", 7, 1),
-    ("e", 3, 1), ("d", 6, 3), ("d", 6, 1), ("d", 7, 2), ("e", 5, 2), ("e", 5, 3), ("e", 3, 2),
-    ("e", 6, 2), ("d", 7, 0), ("d", 7, 3), ("e", 7, 1), ("t", 8), ("e", 6, 1), ("e", 6, 3),
-    ("d", 8, 1), ("d", 5, 0), ("e", 3, 3), ("e", 7, 2), ("e", 7, 3), ("d", 8, 0), ("d", 8, 2),
-    ("d", 8, 3), ("end", 0, 0), ("end", 0, 1), ("end", 0, 2), ("end", 0, 3), ("end", 1, 0),
+    ("own", 0), ("own", 4), ("own", 1), ("norm", 0), ("own", 2), ("norm", 3), ("own", 3),
+    ("norm", 2), ("own", 5), ("a", 3), ("a", 0), ("a", 9), ("own", 6), ("a", 12), ("b", 3),
+    ("b", 0), ("a", 6), ("a", 1), ("norm", 1), ("a", 4), ("odot", 2), ("own", 7), ("odot", 3),
+    ("odot", 1), ("odot", 0), ("odot", 4), ("b", 9), ("odot", 5), ("b", 12), ("odot", 7), ("a", 10),
+    ("c", 0), ("a", 15), ("b", 6), ("c", 3), ("b", 1), ("dot", 0), ("b", 4), ("a", 21), ("a", 13),
+    ("dot", 3), ("c", 9), ("b", 10), ("a", 5), ("c", 12), ("a", 2), ("l", 0), ("b", 15), ("a", 8),
+    ("c", 6), ("c", 1), ("b", 21), ("dot", 6), ("c", 4), ("b", 13), ("a", 7), ("a", 16), ("b", 5),
+    ("b", 2), ("dot", 12), ("b", 8), ("dot", 4), ("t", 0), ("c", 10), ("odot", 6), ("a", 11),
+    ("c", 15), ("c", 21), ("dot", 9), ("a", 19), ("dot", 1), ("a", 14), ("c", 13), ("b", 16),
+    ("b", 7), ("dot", 21), ("a", 23), ("dot", 10), ("b", 11), ("c", 5), ("c", 2), ("a", 17),
+    ("a", 22), ("dot", 15), ("c", 8), ("d", 0, 0), ("b", 14), ("dot", 5), ("l", 2), ("dot", 2),
+    ("l", 1), ("dot", 8), ("c", 7), ("a", 20), ("b", 17), ("d", 0, 1), ("d", 0, 3), ("b", 22),
+    ("d", 0, 2), ("dot", 7), ("l", 3), ("c", 11), ("b", 23), ("b", 19), ("dot", 11), ("l", 4),
+    ("a", 18), ("t", 2), ("b", 20), ("c", 16), ("dot", 13), ("c", 22), ("dot", 16), ("c", 17),
+    ("d", 3, 0), ("d", 1, 0), ("d", 1, 1), ("d", 1, 2), ("c", 19), ("dot", 22), ("dot", 17),
+    ("l", 6), ("t", 4), ("c", 14), ("d", 3, 3), ("b", 18), ("c", 23), ("dot", 19), ("d", 3, 2),
+    ("c", 20), ("d", 3, 1), ("dot", 14), ("l", 5), ("dot", 20), ("e", 3, 2), ("d", 2, 0),
+    ("dot", 23), ("l", 8), ("d", 1, 3), ("e", 1, 2), ("d", 5, 2), ("d", 4, 0), ("t", 6),
+    ("d", 4, 1), ("e", 3, 3), ("c", 18), ("d", 2, 2), ("d", 4, 3), ("dot", 18), ("l", 7),
+    ("d", 2, 1), ("d", 8, 1), ("d", 5, 1), ("d", 5, 3), ("e", 1, 1), ("e", 3, 1), ("d", 8, 2),
+    ("d", 8, 3), ("d", 8, 0), ("e", 1, 3), ("d", 4, 2), ("d", 5, 0), ("d", 7, 2), ("e", 5, 2),
+    ("d", 6, 0), ("d", 7, 1), ("e", 4, 1), ("d", 6, 1), ("d", 2, 3), ("d", 6, 2), ("e", 4, 3),
+    ("d", 7, 0), ("e", 5, 1), ("d", 7, 3), ("d", 6, 3), ("e", 6, 1), ("e", 5, 3), ("e", 8, 3),
+    ("e", 8, 1), ("e", 7, 2), ("e", 4, 2), ("e", 6, 3), ("e", 7, 1), ("e", 8, 2), ("e", 6, 2),
+    ("e", 7, 3), ("end", 0, 0), ("end", 0, 1), ("end", 0, 2), ("end", 0, 3), ("end", 1, 0),
     ("end", 1, 1), ("end", 1, 2), ("end", 1, 3), ("end", 2, 0), ("end", 2, 1), ("end", 2, 2),
     ("end", 2, 3), ("end", 3, 0), ("end", 3, 1), ("end", 3, 2), ("end", 3, 3), ("end", 4, 0),
     ("end", 4, 1), ("end", 4, 2), ("end", 4, 3), ("end", 5, 0), ("end", 5, 1), ("end", 5, 2),
@@ -49,32 +50,33 @@
     ("end", 8, 3),
 )
 MIDDLE = (
-    ("own", 0), ("own", 1), ("norm", 1), ("own", 2), ("norm", 0), ("norm", 2), ("z", 0), ("a", 0),
-    ("z", 1), ("a", 1), ("own", 3), ("z", 4), ("a", 4), ("norm", 3), ("odot", 1), ("odot", 3),
-    ("z", 7), ("a", 7), ("odot", 2), ("odot", 4), ("z", 2), ("a", 2), ("odot", 6), ("b", 1),
-    ("z", 6), ("a", 6), ("z", 3), ("z", 9), ("a", 9), ("a", 3), ("odot", 0), ("z", 10), ("b", 4),
-    ("odot", 7), ("l", 0), ("own", 4), ("a", 10), ("b", 0), ("c", 1), ("z", 5), ("a", 5), ("z", 8),
-    ("a", 8), ("b", 7), ("b", 6), ("b", 3), ("z", 12), ("a", 12), ("z", 13), ("own", 5), ("t", 0),
-    ("a", 13), ("z", 11), ("a", 11), ("b", 9), ("b", 2), ("odot", 5), ("z", 15), ("a", 15),
-    ("c", 4), ("c", 0), ("dot", 0), ("c", 7), ("d", 0, 1), ("b", 10), ("z", 16), ("a", 16),
-    ("dot", 1), ("own", 6), ("z", 14), ("a", 14), ("c", 6), ("b", 5), ("b", 8), ("z", 17),
-    ("dot", 4), ("z", 19), ("own", 7), ("b", 12), ("c", 3), ("c", 2), ("d", 0, 0), ("b", 11),
-    ("d", 0, 2), ("z", 18), ("a", 18), ("dot", 3), ("b", 13), ("a", 17), ("a", 19), ("dot", 6),
-    ("c", 9), ("dot", 2), ("l", 1), ("b", 14), ("c", 10), ("b", 16), ("z", 21), ("a", 21),
-    ("b", 15), ("z", 20), ("a", 20), ("b", 17), ("z", 22), ("a", 22), ("c", 5), ("c", 8), ("z", 23),
-    ("a", 23), ("b", 18), ("dot", 7), ("dot", 5), ("l", 2), ("dot", 8), ("l", 3), ("d", 0, 3),
-    ("c", 11), ("d", 1, 2), ("b", 20), ("dot", 9), ("c", 14), ("dot", 10), ("b", 19), ("dot", 14),
-    ("b", 22), ("c", 12), ("d", 1, 1), ("d", 1, 0), ("dot", 11), ("l", 4), ("c", 13), ("b", 23),
-    ("d", 1, 3), ("b", 21), ("dot", 13), ("d", 3, 2), ("dot", 12), ("l", 5), ("t", 2), ("c", 19),
-    ("c", 16), ("c", 15), ("dot", 15), ("t", 4), ("d", 4, 0), ("c", 17), ("dot", 17), ("d", 3, 1),
-    ("d", 3, 0), ("c", 18), ("dot", 19), ("e", 1, 2), ("d", 5, 2), ("d", 3, 3), ("c", 20),
-    ("d", 2, 0), ("dot", 16), ("l", 6), ("d", 4, 2), ("dot", 18), ("e", 3, 1), ("d", 5, 0),
-    ("e", 1, 1), ("t", 6), ("dot", 20), ("l", 7), ("d", 4, 1), ("c", 22), ("dot", 22), ("d", 4, 3),
-    ("c", 21), ("c", 23), ("d", 5, 1), ("dot", 21), ("d", 2, 2), ("d", 5, 3), ("dot", 23), ("l", 8),
-    ("d", 7, 2), ("e", 1, 3), ("d", 2, 1), ("e", 3, 2), ("d", 2, 3), ("d", 6, 2), ("d", 7, 1),
-    ("d", 7, 3), ("t", 8), ("e", 5, 1), ("e", 5, 3), ("d", 6, 1), ("e", 3, 3), ("e", 5, 2),
-    ("d", 6, 0), ("d", 7, 0), ("e", 7, 2), ("d", 6, 3), ("e", 6, 1), ("e", 6, 2), ("e", 7, 3),
-    ("e", 6, 3), ("d", 8, 1), ("d", 8, 0), ("e", 7, 1), ("d", 8, 3), ("d", 8, 2), ("end", 0, 0),
+    ("own", 0), ("own", 1), ("norm", 0), ("norm", 1), ("own", 2), ("own", 3), ("norm", 3),
+    ("own", 4), ("z", 0), ("a", 0), ("z", 1), ("a", 1), ("z", 4), ("a", 4), ("z", 3), ("a", 3),
+    ("norm", 2), ("odot", 1), ("odot", 6), ("z", 6), ("a", 6), ("z", 7), ("z", 9), ("odot", 3),
+    ("a", 7), ("a", 9), ("z", 10), ("a", 10), ("odot", 4), ("b", 1), ("own", 5), ("b", 4), ("b", 0),
+    ("b", 3), ("odot", 5), ("z", 12), ("own", 7), ("z", 5), ("a", 5), ("b", 7), ("odot", 7),
+    ("z", 13), ("a", 13), ("z", 2), ("a", 2), ("l", 0), ("a", 12), ("b", 10), ("odot", 0), ("b", 9),
+    ("own", 6), ("z", 21), ("z", 8), ("a", 8), ("z", 16), ("a", 16), ("c", 4), ("c", 0), ("z", 15),
+    ("a", 15), ("c", 3), ("dot", 4), ("z", 11), ("a", 11), ("z", 14), ("a", 14), ("odot", 2),
+    ("b", 6), ("z", 19), ("a", 19), ("c", 10), ("dot", 10), ("z", 22), ("a", 22), ("dot", 0),
+    ("c", 1), ("b", 2), ("b", 12), ("z", 17), ("a", 17), ("z", 18), ("a", 18), ("b", 5), ("b", 16),
+    ("b", 8), ("b", 11), ("b", 13), ("c", 9), ("z", 23), ("a", 23), ("b", 22), ("t", 0), ("c", 7),
+    ("b", 15), ("dot", 3), ("c", 2), ("dot", 2), ("c", 6), ("dot", 9), ("c", 5), ("b", 14),
+    ("z", 20), ("a", 21), ("a", 20), ("b", 17), ("b", 18), ("dot", 1), ("l", 1), ("c", 16),
+    ("dot", 16), ("dot", 7), ("b", 19), ("c", 12), ("dot", 5), ("l", 2), ("c", 8), ("b", 20),
+    ("c", 11), ("c", 13), ("b", 23), ("c", 15), ("dot", 15), ("b", 21), ("c", 19), ("dot", 13),
+    ("dot", 6), ("dot", 11), ("l", 4), ("dot", 8), ("l", 3), ("c", 23), ("d", 1, 2), ("t", 2),
+    ("d", 2, 0), ("dot", 19), ("d", 2, 3), ("c", 14), ("c", 17), ("d", 3, 1), ("dot", 12),
+    ("c", 21), ("d", 3, 3), ("dot", 23), ("dot", 14), ("l", 5), ("d", 1, 0), ("d", 1, 3), ("c", 22),
+    ("d", 3, 2), ("e", 3, 1), ("t", 4), ("d", 4, 0), ("c", 18), ("d", 3, 0), ("d", 1, 1),
+    ("d", 0, 3), ("dot", 17), ("l", 6), ("d", 5, 0), ("d", 5, 2), ("c", 20), ("dot", 21),
+    ("dot", 22), ("l", 8), ("dot", 18), ("d", 4, 2), ("d", 2, 2), ("e", 1, 1), ("d", 4, 1),
+    ("t", 6), ("d", 6, 0), ("d", 2, 1), ("e", 1, 3), ("d", 4, 3), ("d", 0, 1), ("dot", 20),
+    ("l", 7), ("d", 5, 1), ("e", 1, 2), ("d", 5, 3), ("e", 5, 1), ("d", 8, 1), ("e", 4, 1),
+    ("d", 6, 2), ("e", 3, 2), ("d", 6, 3), ("d", 0, 0), ("d", 8, 2), ("e", 4, 3), ("d", 7, 2),
+    ("e", 5, 2), ("e", 3, 3), ("d", 6, 1), ("d", 8, 0), ("e", 5, 3), ("d", 0, 2), ("d", 7, 1),
+    ("d", 7, 3), ("e", 7, 1), ("e", 7, 2), ("d", 8, 3), ("e", 6, 2), ("e", 4, 2), ("e", 8, 2),
+    ("e", 7, 3), ("d", 7, 0), ("e", 6, 1), ("e", 8, 1), ("e", 6, 3), ("e", 8, 3), ("end", 0, 0),
     ("end", 0, 1), ("end", 0, 2), ("end", 0, 3), ("end", 1, 0), ("end", 1, 1), ("end", 1, 2),
     ("end", 1, 3), ("end", 2, 0), ("end", 2, 1), ("end", 2, 2), ("end", 2, 3), ("end", 3, 0),
     ("end", 3, 1), ("end", 3, 2), ("end", 3, 3), ("end", 4, 0), ("end", 4, 1), ("end", 4, 2),
@@ -564,7 +566,6 @@
 
 
 def cache_kernel(
-    n_blocks,
     latent_ref,
     gain_ref,
     wk_ref,
@@ -572,21 +573,30 @@
     q_nope_ref,
     q_rope_ref,
     rope_ref,
-    keys_ref,
-    values_ref,
+    keys_hbm,
+    values_hbm,
     rope_keys_ref,
     read_ref,
-    scores,
-    held,
+    latents,
+    keys,
+    values,
+    sems,
 ):
-    b = pl.program_id(0)
-    heads = scores.shape[1]
+    n_blocks, rows, out_cols = keys.shape
+    heads = out_cols // HEAD
 
     def per_head(row, size):
         wide = jnp.broadcast_to(row.astype(jnp.float32), (heads, heads * size))
         head = lax.broadcasted_iota(jnp.int32, wide.shape, 0)
         lane = lax.broadcasted_iota(jnp.int32, wide.shape, 1)
         return jnp.where((lane >= head * size) & (lane < head * size + size), wide, 0.0)
+
+    def put(b, source, target, kind):
+        copy = pltpu.make_async_copy(
+            source.at[b], target.at[pl.ds(b * rows, rows), :], sems.at[kind, b]
+        )
+        copy.start()
+        return copy
 
     query = per_head(q_nope_ref[...], HEAD).astype(jnp.bfloat16)
     spread = (heads * ROPE, ROPE)
@@ -598,72 +608,77 @@
         jnp.where(fold, 1.0, 0.0).astype(jnp.bfloat16),
         preferred_element_type=jnp.float32,
     ).astype(jnp.bfloat16)
-    raw = latent_ref[0].astype(jnp.float32)
-    scale = lax.rsqrt(jnp.mean(raw * raw, axis=-1, keepdims=True) + EPS)
-    latent = (raw * scale * gain_ref[...]).astype(jnp.bfloat16)
-    keys = jnp.dot(latent, wk_ref[...], preferred_element_type=jnp.float32).astype(jnp.bfloat16)
-    keys_ref[...] = keys
-    values = jnp.dot(latent, wv_ref[...], preferred_element_type=jnp.float32).astype(jnp.bfloat16)
-    values_ref[...] = values
-    held[b] = values
-    rope = rope_ref[0]
-    rope_keys_ref[...] = rope
     across = (((1,), (1,)), ((), ()))
-    part = lax.dot_general(query, keys, across, preferred_element_type=jnp.float32)
-    part += jnp.dot(rotary_q, rope, preferred_element_type=jnp.float32)
-    scores[b] = part / jnp.sqrt(jnp.float32(HEAD + ROPE))
-
-    @pl.when(b == n_blocks - 1)
-    def _():
-        every = scores[...]
-        peak = jnp.max(jnp.max(every, axis=-1, keepdims=True), axis=0, keepdims=True)
-        expo = jnp.exp(every - peak)
-        total = jnp.sum(jnp.sum(expo, axis=-1, keepdims=True), axis=0, keepdims=True)
-        weights = (expo / total).astype(jnp.bfloat16)
-        out = jnp.dot(weights[0], held[0], preferred_element_type=jnp.float32)
-        for i in range(1, n_blocks):
-            out += jnp.dot(weights[i], held[i], preferred_element_type=jnp.float32)
-        head = lax.broadcasted_iota(jnp.int32, out.shape, 0)
-        lane = lax.broadcasted_iota(jnp.int32, out.shape, 1)
-        picked = jnp.where((lane >= head * HEAD) & (lane < head * HEAD + HEAD), out, 0.0)
-        read_ref[...] = jnp.sum(picked, axis=0, keepdims=True).astype(jnp.bfloat16)
+    copies, scores = [], []
+
+    def normalize(b):
+        raw = latent_ref[b].astype(jnp.float32)
+        scale = lax.rsqrt(jnp.mean(raw * raw, axis=-1, keepdims=True) + EPS)
+        latents[b] = (raw * scale * gain_ref[...]).astype(jnp.bfloat16)
+
+    def up_key(b):
+        block = jnp.dot(latents[b], wk_ref[...], preferred_element_type=jnp.float32)
+        keys[b] = block.astype(jnp.bfloat16)
+        copies.append(put(b, keys, keys_hbm, 0))
+
+    def up_value(b):
+        block = jnp.dot(latents[b], wv_ref[...], preferred_element_type=jnp.float32)
+        values[b] = block.astype(jnp.bfloat16)
+        copies.append(put(b, values, values_hbm, 1))
+
+    def score(b):
+        part = lax.dot_general(query, keys[b], across, preferred_element_type=jnp.float32)
+        part += jnp.dot(rotary_q, rope_ref[b], preferred_element_type=jnp.float32)
+        scores.append(part / jnp.sqrt(jnp.float32(HEAD + ROPE)))
+        rope_keys_ref[:, b * rows : (b + 1) * rows] = rope_ref[b]
+
+    normalize(0)
+    for b in range(n_blocks):
+        if b + 1 < n_blocks:
+            normalize(b + 1)
+        up_key(b)
+        if b + 1 < n_blocks:
+            up_value(b)
+        score(b)
+    up_value(n_blocks - 1)
+    peak = functools.reduce(jnp.maximum, scores).max(axis=-1, keepdims=True)
+    expos = [jnp.exp(part - peak) for part in scores]
+    total = functools.reduce(jnp.add, expos).sum(axis=-1, keepdims=True)
+    out = jnp.zeros((heads, out_cols), jnp.float32)
+    for b in range(n_blocks):
+        weights = (expos[b] / total).astype(jnp.bfloat16)
+        out += jnp.dot(weights, values[b], preferred_element_type=jnp.float32)
+    head = lax.broadcasted_iota(jnp.int32, out.shape, 0)
+    lane = lax.broadcasted_iota(jnp.int32, out.shape, 1)
+    picked = jnp.where((lane >= head * HEAD) & (lane < head * HEAD + HEAD), out, 0.0)
+    read_ref[...] = jnp.sum(picked, axis=0, keepdims=True).astype(jnp.bfloat16)
+    for copy in copies:
+        copy.wait()
 
 
 def fill_cache(latent, kv_gain, w_up_key, w_up_value, q_nope, q_rope, rope):
     n_blocks, rows, cols = latent.shape
     out_cols = w_up_key.shape[1]
-    heads = out_cols // HEAD
     length = n_blocks * rows
-    whole = lambda shape: pl.BlockSpec(shape, lambda b: (0,) * len(shape))
+    vmem = pl.BlockSpec(memory_space=pltpu.VMEM)
+    hbm = pl.BlockSpec(memory_space=pltpu.HBM)
     return pl.pallas_call(
-        functools.partial(cache_kernel, n_blocks),
-        grid=(n_blocks,),
+        cache_kernel,
         out_shape=(
             jax.ShapeDtypeStruct((length, out_cols), jnp.bfloat16),
             jax.ShapeDtypeStruct((length, out_cols), jnp.bfloat16),
             jax.ShapeDtypeStruct((ROPE, length), jnp.bfloat16),
             jax.ShapeDtypeStruct((1, out_cols), jnp.bfloat16),
         ),
-        in_specs=[
-            pl.BlockSpec((1, rows, cols), lambda b: (b, 0, 0)),
-            whole((1, cols)),
-            whole((cols, out_cols)),
-            whole((cols, out_cols)),
-            whole(q_nope.shape),
-            whole(q_rope.shape),
-            pl.BlockSpec((1, ROPE, rows), lambda b: (b, 0, 0)),
+        in_specs=[vmem] * 7,
+        out_specs=(hbm, hbm, vmem, vmem),
+        scratch_shapes=[
+            pltpu.VMEM((n_blocks, rows, cols), jnp.bfloat16),
+            pltpu.VMEM((n_blocks, rows, out_cols), jnp.bfloat16),
+            pltpu.VMEM((n_blocks, rows, out_cols), jnp.bfloat16),
+            pltpu.SemaphoreType.DMA((2, n_blocks)),
         ],
-        out_specs=(
-            pl.BlockSpec((rows, out_cols), lambda b: (b, 0)),
-            pl.BlockSpec((rows, out_cols), lambda b: (b, 0)),
-            pl.BlockSpec((ROPE, rows), lambda b: (0, b)),
-            whole((1, out_cols)),
-        ),
-        scratch_shapes=[
-            pltpu.VMEM((n_blocks, heads, rows), jnp.float32),
-            pltpu.VMEM((n_blocks, rows, out_cols), jnp.bfloat16),
-        ],
-        compiler_params=pltpu.CompilerParams(vmem_limit_bytes=30 * 1024 * 1024),
+        compiler_params=pltpu.CompilerParams(vmem_limit_bytes=40 * 1024 * 1024),
     )(latent, kv_gain, w_up_key, w_up_value, q_nope, q_rope, rope)
 
 

time: 68.8 us -> 64.7 us (0.940)
  Pallas kernels: 67.1 us -> 63 us
    pallas_call x1, Pallas kernels: 62.4 us -> 58.4 us  [gather_latent(): pl.pallas_call(functools.partial(gather_kernel, n_grp, n_sp, n_tp, spans,...]
where the time goes in v2:
time: 64.7 us; the launch traced here: 64.5 us
  Pallas kernels  63 us (97%)
  between operations  1.55 us (2%)
    pallas_call x1, Pallas kernels, gather_latent(): pl.pallas_call(functools.partial(gather_kernel, n_grp, n_sp, n_tp, spans,...  58.4 us
    pallas_call x1, Pallas kernels, fill_cache(): pl.pallas_call(cache_kernel, out_shape=(jax.ShapeDtypeStruct((length, out...  4.54 us

profile of v2, /device:TPU:1, one launch (start us, length us, event | category | flops | bytes accessed | tf_op | source)
XLA Modules:
  0.0 64.5 jit_solution(11623034054302423917)
XLA Ops:
  1.3 0.0 copy-start
  1.3 0.0 copy-start.1
  1.3 0.0 copy-start.2
  1.3 0.0 copy-start.3
  1.3 0.0 copy-start.4
  1.3 58.4 %shard_map.129 = (bf16[4,256,1024]{2,1,0:T(8,128)(2,1)S(1)}, bf16[4,32,256]{2,1,0:T(8,128)(2,1)S(1)}) custom-call(bf16[256,4096]{1,0:T(8,128)(2,1)} %bitcast.8, bf16[1024,1024]{1,0:T(8,128)(2,1)} %refs_1_.1, bf16[32,4096]{1,0:T(8,128)(2,1)} %bitcast.9, f32[1,4096]{1,0:T(1,128)} %bitcast.10, s32[1]{0:T(128)S(6)} %copy.14.refs_4_), custom_call_target="tpu_custom_call" | custom-call | tf_op jit(solution)/shard_map/pallas_call | solution.py:524
  59.8 0.0 copy-done
  59.8 0.0 copy-done.1
  59.8 0.0 copy-done.2
  59.8 0.0 copy-done.3
  59.8 0.0 copy-done.4
  59.8 4.5 %shard_map.130 = (bf16[1024,512]{1,0:T(8,128)(2,1)}, bf16[1024,512]{1,0:T(8,128)(2,1)}, bf16[32,1024]{1,0:T(8,128)(2,1)}, bf16[1,512]{1,0:T(2,128)(2,1)}) custom-call(bf16[4,256,1024]{2,1,0:T(8,128)(2,1)S(1)} %get-tuple-element.10.latent_ref, f32[1,1024]{1,0:T(1,128)S(1)} %bitcast.7, bf16[1024,512]{1,0:T(8,128)(2,1)S(1)} %copy-done, ...), custom_call_target="tpu_custom_call" | custom-call | tf_op jit(solution)/shard_map/pallas_call | solution.py:665
Async XLA Ops:
  1.3 58.5 %copy-start = (bf16[1024,512]{1,0:T(8,128)(2,1)S(1)}, bf16[1024,512]{1,0:T(8,128)(2,1)}, u32[]{:S(2)}) copy-start(bf16[1024,512]{1,0:T(8,128)(2,1)} %wk_ref.1) | copy-start | bytes 3145732
  1.3 58.5 %copy-start.1 = (bf16[1024,512]{1,0:T(8,128)(2,1)S(1)}, bf16[1024,512]{1,0:T(8,128)(2,1)}, u32[]{:S(2)}) copy-start(bf16[1024,512]{1,0:T(8,128)(2,1)} %wv_ref.1) | copy-start | bytes 3145732
  1.3 58.5 %copy-start.2 = (f32[1024]{0:T(1024)S(1)}, f32[1024]{0:T(1024)}, u32[]{:S(2)}) copy-start(f32[1024]{0:T(1024)} %param.15) | copy-start | bytes 12292
  1.3 58.5 %copy-start.3 = (bf16[1,512]{1,0:T(2,128)(2,1)S(1)}, bf16[1,512]{1,0:T(2,128)(2,1)}, u32[]{:S(2)}) copy-start(bf16[1,512]{1,0:T(2,128)(2,1)} %q_nope_ref.1) | copy-start | bytes 3076
  1.3 58.5 %copy-start.4 = (bf16[1,256]{1,0:T(2,128)(2,1)S(1)}, bf16[1,256]{1,0:T(2,128)(2,1)}, u32[]{:S(2)}) copy-start(bf16[1,256]{1,0:T(2,128)(2,1)} %q_rope_ref.1) | copy-start | bytes 1540

commit v3 on v2

--- a/solution.py
+++ b/solution.py
@@ -14,75 +14,75 @@
 PIECES = 4
 PENDING = 60
 PARTS = (1, 1, 1, 1, 1, 1, 1, 1)
-MODES = ("F", "O", "F", "O", "C", "O", "C", "O", "O")
-X_FIRST = (True, False, False, False, True, True, True, False, True, True, True, True, False, True, True, False, True, True, False, False, True, True, True, False)
+MODES = ("M", "F", "M", "M", "F", "M", "F", "O", "F")
+DOUBLED = (False, False, False, False, True, False, True, True)
+X_FIRST = (False, True, True, True, True, True, True, False, True, False, True, True, False, False, True, False, True, True, False, False, True, False, True, True)
 OUTER = (
-    ("own", 0), ("own", 4), ("own", 1), ("norm", 0), ("own", 2), ("norm", 3), ("own", 3),
-    ("norm", 2), ("own", 5), ("a", 3), ("a", 0), ("a", 9), ("own", 6), ("a", 12), ("b", 3),
-    ("b", 0), ("a", 6), ("a", 1), ("norm", 1), ("a", 4), ("odot", 2), ("own", 7), ("odot", 3),
-    ("odot", 1), ("odot", 0), ("odot", 4), ("b", 9), ("odot", 5), ("b", 12), ("odot", 7), ("a", 10),
-    ("c", 0), ("a", 15), ("b", 6), ("c", 3), ("b", 1), ("dot", 0), ("b", 4), ("a", 21), ("a", 13),
-    ("dot", 3), ("c", 9), ("b", 10), ("a", 5), ("c", 12), ("a", 2), ("l", 0), ("b", 15), ("a", 8),
-    ("c", 6), ("c", 1), ("b", 21), ("dot", 6), ("c", 4), ("b", 13), ("a", 7), ("a", 16), ("b", 5),
-    ("b", 2), ("dot", 12), ("b", 8), ("dot", 4), ("t", 0), ("c", 10), ("odot", 6), ("a", 11),
-    ("c", 15), ("c", 21), ("dot", 9), ("a", 19), ("dot", 1), ("a", 14), ("c", 13), ("b", 16),
-    ("b", 7), ("dot", 21), ("a", 23), ("dot", 10), ("b", 11), ("c", 5), ("c", 2), ("a", 17),
-    ("a", 22), ("dot", 15), ("c", 8), ("d", 0, 0), ("b", 14), ("dot", 5), ("l", 2), ("dot", 2),
-    ("l", 1), ("dot", 8), ("c", 7), ("a", 20), ("b", 17), ("d", 0, 1), ("d", 0, 3), ("b", 22),
-    ("d", 0, 2), ("dot", 7), ("l", 3), ("c", 11), ("b", 23), ("b", 19), ("dot", 11), ("l", 4),
-    ("a", 18), ("t", 2), ("b", 20), ("c", 16), ("dot", 13), ("c", 22), ("dot", 16), ("c", 17),
-    ("d", 3, 0), ("d", 1, 0), ("d", 1, 1), ("d", 1, 2), ("c", 19), ("dot", 22), ("dot", 17),
-    ("l", 6), ("t", 4), ("c", 14), ("d", 3, 3), ("b", 18), ("c", 23), ("dot", 19), ("d", 3, 2),
-    ("c", 20), ("d", 3, 1), ("dot", 14), ("l", 5), ("dot", 20), ("e", 3, 2), ("d", 2, 0),
-    ("dot", 23), ("l", 8), ("d", 1, 3), ("e", 1, 2), ("d", 5, 2), ("d", 4, 0), ("t", 6),
-    ("d", 4, 1), ("e", 3, 3), ("c", 18), ("d", 2, 2), ("d", 4, 3), ("dot", 18), ("l", 7),
-    ("d", 2, 1), ("d", 8, 1), ("d", 5, 1), ("d", 5, 3), ("e", 1, 1), ("e", 3, 1), ("d", 8, 2),
-    ("d", 8, 3), ("d", 8, 0), ("e", 1, 3), ("d", 4, 2), ("d", 5, 0), ("d", 7, 2), ("e", 5, 2),
-    ("d", 6, 0), ("d", 7, 1), ("e", 4, 1), ("d", 6, 1), ("d", 2, 3), ("d", 6, 2), ("e", 4, 3),
-    ("d", 7, 0), ("e", 5, 1), ("d", 7, 3), ("d", 6, 3), ("e", 6, 1), ("e", 5, 3), ("e", 8, 3),
-    ("e", 8, 1), ("e", 7, 2), ("e", 4, 2), ("e", 6, 3), ("e", 7, 1), ("e", 8, 2), ("e", 6, 2),
-    ("e", 7, 3), ("end", 0, 0), ("end", 0, 1), ("end", 0, 2), ("end", 0, 3), ("end", 1, 0),
-    ("end", 1, 1), ("end", 1, 2), ("end", 1, 3), ("end", 2, 0), ("end", 2, 1), ("end", 2, 2),
-    ("end", 2, 3), ("end", 3, 0), ("end", 3, 1), ("end", 3, 2), ("end", 3, 3), ("end", 4, 0),
-    ("end", 4, 1), ("end", 4, 2), ("end", 4, 3), ("end", 5, 0), ("end", 5, 1), ("end", 5, 2),
-    ("end", 5, 3), ("end", 6, 0), ("end", 6, 1), ("end", 6, 2), ("end", 6, 3), ("end", 7, 0),
-    ("end", 7, 1), ("end", 7, 2), ("end", 7, 3), ("end", 8, 0), ("end", 8, 1), ("end", 8, 2),
-    ("end", 8, 3),
+    ("own", 2), ("norm", 1), ("own", 0), ("own", 1), ("norm", 2), ("norm", 0), ("norm", 3),
+    ("odot", 0), ("odot", 5), ("a", 3), ("a", 6), ("a", 0), ("odot", 6), ("odot", 1), ("odot", 2),
+    ("odot", 7), ("odot", 3), ("own", 3), ("own", 4), ("b", 3), ("b", 6), ("b", 0), ("a", 7),
+    ("own", 5), ("a", 1), ("a", 9), ("a", 4), ("c", 0), ("a", 2), ("odot", 4), ("own", 6), ("l", 0),
+    ("a", 12), ("b", 1), ("b", 9), ("b", 4), ("own", 7), ("a", 5), ("c", 3), ("a", 10), ("a", 8),
+    ("a", 15), ("c", 6), ("dot", 0), ("dot", 3), ("b", 7), ("c", 9), ("b", 2), ("t", 0), ("a", 13),
+    ("b", 13), ("c", 1), ("a", 11), ("b", 12), ("c", 12), ("c", 4), ("d", 0, 2), ("dot", 6),
+    ("dot", 9), ("a", 18), ("b", 10), ("d", 0, 0), ("b", 15), ("b", 5), ("dot", 1), ("d", 0, 1),
+    ("b", 18), ("dot", 12), ("b", 8), ("dot", 4), ("c", 7), ("a", 14), ("c", 2), ("a", 16),
+    ("dot", 7), ("d", 0, 3), ("b", 11), ("e", 0, 2), ("c", 13), ("dot", 13), ("a", 21), ("a", 19),
+    ("c", 10), ("a", 17), ("c", 15), ("dot", 2), ("l", 1), ("b", 16), ("e", 0, 3), ("e", 0, 1),
+    ("c", 5), ("b", 21), ("c", 8), ("a", 22), ("dot", 10), ("dot", 5), ("l", 2), ("c", 11),
+    ("dot", 8), ("l", 3), ("dot", 15), ("a", 20), ("c", 18), ("t", 1), ("b", 17), ("c", 21),
+    ("dot", 18), ("b", 14), ("c", 14), ("dot", 11), ("l", 4), ("b", 20), ("t", 3), ("a", 23),
+    ("dot", 14), ("l", 5), ("b", 19), ("c", 19), ("c", 20), ("d", 3, 0), ("dot", 21), ("t", 2),
+    ("c", 16), ("dot", 16), ("c", 17), ("d", 2, 2), ("d", 2, 0), ("dot", 20), ("b", 23), ("c", 23),
+    ("d", 1, 1), ("t", 5), ("t", 4), ("dot", 19), ("l", 7), ("d", 1, 0), ("d", 4, 0), ("d", 3, 3),
+    ("dot", 17), ("l", 6), ("dot", 23), ("d", 5, 0), ("d", 2, 3), ("d", 1, 2), ("b", 22), ("c", 22),
+    ("d", 5, 3), ("d", 2, 1), ("e", 2, 2), ("dot", 22), ("l", 8), ("d", 3, 1), ("d", 5, 1),
+    ("d", 5, 2), ("d", 4, 1), ("d", 3, 2), ("e", 3, 1), ("e", 3, 3), ("d", 1, 3), ("d", 7, 3),
+    ("e", 2, 1), ("d", 4, 3), ("d", 4, 2), ("d", 7, 0), ("d", 7, 2), ("t", 6), ("d", 6, 1),
+    ("d", 6, 2), ("d", 7, 1), ("d", 6, 3), ("d", 6, 0), ("e", 7, 3), ("e", 5, 1), ("e", 2, 3),
+    ("t", 8), ("e", 7, 1), ("e", 5, 3), ("e", 3, 2), ("e", 5, 2), ("d", 8, 1), ("e", 7, 2),
+    ("d", 8, 0), ("d", 8, 2), ("d", 8, 3), ("end", 0, 0), ("end", 0, 1), ("end", 0, 2),
+    ("end", 0, 3), ("end", 1, 0), ("end", 1, 1), ("end", 1, 2), ("end", 1, 3), ("end", 2, 0),
+    ("end", 2, 1), ("end", 2, 2), ("end", 2, 3), ("end", 3, 0), ("end", 3, 1), ("end", 3, 2),
+    ("end", 3, 3), ("end", 4, 0), ("end", 4, 1), ("end", 4, 2), ("end", 4, 3), ("end", 5, 0),
+    ("end", 5, 1), ("end", 5, 2), ("end", 5, 3), ("end", 6, 0), ("end", 6, 1), ("end", 6, 2),
+    ("end", 6, 3), ("end", 7, 0), ("end", 7, 1), ("end", 7, 2), ("end", 7, 3), ("end", 8, 0),
+    ("end", 8, 1), ("end", 8, 2), ("end", 8, 3),
 )
 MIDDLE = (
-    ("own", 0), ("own", 1), ("norm", 0), ("norm", 1), ("own", 2), ("own", 3), ("norm", 3),
-    ("own", 4), ("z", 0), ("a", 0), ("z", 1), ("a", 1), ("z", 4), ("a", 4), ("z", 3), ("a", 3),
-    ("norm", 2), ("odot", 1), ("odot", 6), ("z", 6), ("a", 6), ("z", 7), ("z", 9), ("odot", 3),
-    ("a", 7), ("a", 9), ("z", 10), ("a", 10), ("odot", 4), ("b", 1), ("own", 5), ("b", 4), ("b", 0),
-    ("b", 3), ("odot", 5), ("z", 12), ("own", 7), ("z", 5), ("a", 5), ("b", 7), ("odot", 7),
-    ("z", 13), ("a", 13), ("z", 2), ("a", 2), ("l", 0), ("a", 12), ("b", 10), ("odot", 0), ("b", 9),
-    ("own", 6), ("z", 21), ("z", 8), ("a", 8), ("z", 16), ("a", 16), ("c", 4), ("c", 0), ("z", 15),
-    ("a", 15), ("c", 3), ("dot", 4), ("z", 11), ("a", 11), ("z", 14), ("a", 14), ("odot", 2),
-    ("b", 6), ("z", 19), ("a", 19), ("c", 10), ("dot", 10), ("z", 22), ("a", 22), ("dot", 0),
-    ("c", 1), ("b", 2), ("b", 12), ("z", 17), ("a", 17), ("z", 18), ("a", 18), ("b", 5), ("b", 16),
-    ("b", 8), ("b", 11), ("b", 13), ("c", 9), ("z", 23), ("a", 23), ("b", 22), ("t", 0), ("c", 7),
-    ("b", 15), ("dot", 3), ("c", 2), ("dot", 2), ("c", 6), ("dot", 9), ("c", 5), ("b", 14),
-    ("z", 20), ("a", 21), ("a", 20), ("b", 17), ("b", 18), ("dot", 1), ("l", 1), ("c", 16),
-    ("dot", 16), ("dot", 7), ("b", 19), ("c", 12), ("dot", 5), ("l", 2), ("c", 8), ("b", 20),
-    ("c", 11), ("c", 13), ("b", 23), ("c", 15), ("dot", 15), ("b", 21), ("c", 19), ("dot", 13),
-    ("dot", 6), ("dot", 11), ("l", 4), ("dot", 8), ("l", 3), ("c", 23), ("d", 1, 2), ("t", 2),
-    ("d", 2, 0), ("dot", 19), ("d", 2, 3), ("c", 14), ("c", 17), ("d", 3, 1), ("dot", 12),
-    ("c", 21), ("d", 3, 3), ("dot", 23), ("dot", 14), ("l", 5), ("d", 1, 0), ("d", 1, 3), ("c", 22),
-    ("d", 3, 2), ("e", 3, 1), ("t", 4), ("d", 4, 0), ("c", 18), ("d", 3, 0), ("d", 1, 1),
-    ("d", 0, 3), ("dot", 17), ("l", 6), ("d", 5, 0), ("d", 5, 2), ("c", 20), ("dot", 21),
-    ("dot", 22), ("l", 8), ("dot", 18), ("d", 4, 2), ("d", 2, 2), ("e", 1, 1), ("d", 4, 1),
-    ("t", 6), ("d", 6, 0), ("d", 2, 1), ("e", 1, 3), ("d", 4, 3), ("d", 0, 1), ("dot", 20),
-    ("l", 7), ("d", 5, 1), ("e", 1, 2), ("d", 5, 3), ("e", 5, 1), ("d", 8, 1), ("e", 4, 1),
-    ("d", 6, 2), ("e", 3, 2), ("d", 6, 3), ("d", 0, 0), ("d", 8, 2), ("e", 4, 3), ("d", 7, 2),
-    ("e", 5, 2), ("e", 3, 3), ("d", 6, 1), ("d", 8, 0), ("e", 5, 3), ("d", 0, 2), ("d", 7, 1),
-    ("d", 7, 3), ("e", 7, 1), ("e", 7, 2), ("d", 8, 3), ("e", 6, 2), ("e", 4, 2), ("e", 8, 2),
-    ("e", 7, 3), ("d", 7, 0), ("e", 6, 1), ("e", 8, 1), ("e", 6, 3), ("e", 8, 3), ("end", 0, 0),
-    ("end", 0, 1), ("end", 0, 2), ("end", 0, 3), ("end", 1, 0), ("end", 1, 1), ("end", 1, 2),
-    ("end", 1, 3), ("end", 2, 0), ("end", 2, 1), ("end", 2, 2), ("end", 2, 3), ("end", 3, 0),
-    ("end", 3, 1), ("end", 3, 2), ("end", 3, 3), ("end", 4, 0), ("end", 4, 1), ("end", 4, 2),
-    ("end", 4, 3), ("end", 5, 0), ("end", 5, 1), ("end", 5, 2), ("end", 5, 3), ("end", 6, 0),
-    ("end", 6, 1), ("end", 6, 2), ("end", 6, 3), ("end", 7, 0), ("end", 7, 1), ("end", 7, 2),
-    ("end", 7, 3), ("end", 8, 0), ("end", 8, 1), ("end", 8, 2), ("end", 8, 3),
+    ("own", 0), ("norm", 0), ("own", 1), ("norm", 1), ("own", 2), ("norm", 2), ("norm", 3),
+    ("z", 6), ("z", 1), ("z", 0), ("own", 3), ("z", 4), ("z", 3), ("z", 7), ("a", 1), ("odot", 5),
+    ("odot", 0), ("a", 3), ("odot", 1), ("odot", 2), ("a", 0), ("odot", 4), ("odot", 7), ("own", 4),
+    ("a", 6), ("odot", 3), ("odot", 6), ("z", 2), ("b", 1), ("b", 0), ("z", 9), ("b", 3), ("z", 5),
+    ("a", 7), ("a", 2), ("l", 0), ("own", 5), ("z", 10), ("z", 8), ("a", 4), ("a", 9), ("c", 1),
+    ("c", 0), ("a", 5), ("z", 13), ("z", 12), ("a", 10), ("a", 12), ("b", 12), ("a", 8), ("a", 13),
+    ("b", 13), ("b", 6), ("z", 11), ("own", 6), ("c", 3), ("t", 0), ("d", 0, 0), ("b", 7),
+    ("z", 15), ("b", 2), ("a", 11), ("dot", 3), ("b", 4), ("z", 16), ("own", 7), ("dot", 1),
+    ("dot", 0), ("b", 9), ("c", 6), ("b", 5), ("d", 0, 3), ("z", 14), ("a", 16), ("c", 7), ("c", 4),
+    ("c", 2), ("b", 10), ("z", 21), ("a", 15), ("z", 19), ("b", 8), ("c", 12), ("c", 13), ("z", 17),
+    ("a", 14), ("b", 14), ("b", 11), ("dot", 4), ("z", 22), ("a", 17), ("c", 9), ("d", 0, 2),
+    ("z", 18), ("a", 19), ("b", 19), ("a", 18), ("dot", 7), ("dot", 2), ("l", 1), ("c", 10),
+    ("d", 0, 1), ("z", 20), ("b", 15), ("dot", 13), ("c", 5), ("dot", 9), ("b", 16), ("b", 18),
+    ("dot", 12), ("e", 0, 3), ("dot", 5), ("l", 2), ("dot", 6), ("c", 8), ("a", 22), ("a", 20),
+    ("b", 20), ("t", 1), ("e", 0, 2), ("c", 14), ("c", 11), ("a", 21), ("z", 23), ("a", 23),
+    ("c", 19), ("b", 21), ("b", 17), ("dot", 10), ("c", 18), ("dot", 8), ("l", 3), ("dot", 14),
+    ("l", 5), ("c", 16), ("b", 22), ("e", 0, 1), ("c", 15), ("dot", 11), ("l", 4), ("dot", 19),
+    ("b", 23), ("c", 21), ("c", 22), ("c", 23), ("t", 3), ("dot", 15), ("c", 20), ("dot", 16),
+    ("c", 17), ("dot", 21), ("d", 3, 3), ("d", 3, 0), ("t", 2), ("d", 2, 0), ("d", 2, 1),
+    ("d", 2, 3), ("dot", 20), ("dot", 18), ("l", 7), ("d", 3, 2), ("dot", 17), ("l", 6),
+    ("d", 3, 1), ("t", 4), ("d", 4, 0), ("d", 1, 2), ("d", 1, 0), ("d", 2, 2), ("e", 2, 3),
+    ("dot", 22), ("t", 5), ("d", 5, 0), ("d", 1, 1), ("d", 7, 0), ("d", 1, 3), ("d", 5, 2),
+    ("dot", 23), ("l", 8), ("d", 5, 1), ("d", 4, 2), ("d", 4, 1), ("e", 3, 1), ("d", 7, 1),
+    ("e", 2, 2), ("e", 3, 2), ("e", 2, 1), ("d", 5, 3), ("t", 6), ("d", 6, 1), ("d", 7, 3),
+    ("t", 8), ("d", 7, 2), ("e", 7, 1), ("e", 7, 3), ("d", 6, 2), ("e", 5, 3), ("e", 3, 3),
+    ("d", 4, 3), ("e", 5, 2), ("e", 5, 1), ("d", 6, 3), ("d", 6, 0), ("e", 7, 2), ("d", 8, 2),
+    ("d", 8, 1), ("d", 8, 3), ("d", 8, 0), ("end", 0, 0), ("end", 0, 1), ("end", 0, 2),
+    ("end", 0, 3), ("end", 1, 0), ("end", 1, 1), ("end", 1, 2), ("end", 1, 3), ("end", 2, 0),
+    ("end", 2, 1), ("end", 2, 2), ("end", 2, 3), ("end", 3, 0), ("end", 3, 1), ("end", 3, 2),
+    ("end", 3, 3), ("end", 4, 0), ("end", 4, 1), ("end", 4, 2), ("end", 4, 3), ("end", 5, 0),
+    ("end", 5, 1), ("end", 5, 2), ("end", 5, 3), ("end", 6, 0), ("end", 6, 1), ("end", 6, 2),
+    ("end", 6, 3), ("end", 7, 0), ("end", 7, 1), ("end", 7, 2), ("end", 7, 3), ("end", 8, 0),
+    ("end", 8, 1), ("end", 8, 2), ("end", 8, 3),
 )
 
 EPS = 1e-06
@@ -183,6 +183,7 @@
 
     finish, fetched = [], []
     tuned = n_sp == 4 and groups == len(PARTS)
+    doubled = DOUBLED if tuned and n_x == 2 and n_grp == 2 else (False,) * groups
     modes = MODES if tuned else ("F",) * (groups + 1)
 
     def remote(src, dst, send, recv, device):
@@ -223,17 +224,24 @@
 
     shards = {d: shard(d) for d in range(1, n_sp)}
 
+    def corners(g):
+        here = [(rank, x, y)]
+        if doubled[g]:
+            here.append(((core * n_x + 1 - x) * n_grp + 1 - y, 1 - x, 1 - y))
+        return list(enumerate(here))
+
     def own_z(g):
         first, width = spans[g]
         for side, ahead, exists in ((0, z_up, has_up), (1, z_down, has_down)):
-            copy = remote(
-                w_hbm.at[pl.ds(rank * chunk, chunk), pl.ds(first, width)],
-                wbuf[g].at[z, core, x, y],
-                own_send.at[g, side],
-                z_recv.at[g, z],
-                {"sp": ahead},
-            )
-            begin(copy, exists)
+            for q, (index, at_x, at_y) in corners(g):
+                copy = remote(
+                    w_hbm.at[pl.ds(index * chunk, chunk), pl.ds(first, width)],
+                    wbuf[g].at[z, core, at_x, at_y],
+                    own_send.at[g, side, q],
+                    z_recv.at[g, z, q],
+                    {"sp": ahead},
+                )
+                begin(copy, exists)
 
     def x_first(u):
         return X_FIRST[u] if tuned else u % 4 > 0
@@ -257,25 +265,35 @@
     def stage_z(u):
         g, d = units[u]
         s, up = shards[d]
-        arrived(block_a(u), z_recv.at[g, s])
         exists = jnp.where(up, has_down, has_up)
         ahead = jnp.where(up, z_down, z_up)
-        begin(
-            remote(block_a(u), block_a(u), z_send.at[u], z_recv.at[g, s], {"sp": ahead}), exists
-        )
+        for q, (_, at_x, at_y) in corners(g):
+            block = wbuf[g].at[s, core, at_x, at_y]
+            arrived(block, z_recv.at[g, s, q])
+            begin(remote(block, block, z_send.at[u, q], z_recv.at[g, s, q], {"sp": ahead}), exists)
 
     def stage_a(u):
-        spread(u, block_a(u), a_send, a_recv, x_first(u))
+        if doubled[units[u][0]]:
+            spread(u, block_a(u), a_send, a_recv, True)
+            spread(u, block_a(u), b_send, b_recv, False)
+        else:
+            spread(u, block_a(u), a_send, a_recv, x_first(u))
 
     def stage_b(u):
+        if doubled[units[u][0]]:
+            return
         for k in range(len(x_peers if x_first(u) else y_peers)):
             arrived(block_a(u), a_recv.at[u, k])
         spread(u, block_b(u), b_send, b_recv, not x_first(u))
 
     def stage_c(u):
         g, d = units[u]
-        for k in range(len(y_peers if x_first(u) else x_peers)):
-            arrived(block_b(u), b_recv.at[u, k])
+        if doubled[g]:
+            arrived(block_a(u), a_recv.at[u, 0])
+            arrived(block_a(u), b_recv.at[u, 0])
+        else:
+            for k in range(len(y_peers if x_first(u) else x_peers)):
+                arrived(block_b(u), b_recv.at[u, k])
         ref = wbuf[g].at[shards[d][0], core]
         begin(remote(ref, ref, c_send.at[u], c_recv.at[u], partner))
 
@@ -298,40 +316,53 @@
     def held(m, k, i):
         return transit_rope.at[k, i] if m == 0 else transit[m - 1].at[k, i]
 
+    def own_line(m, source, home):
+        if modes[m] == "M":
+            return (source + home + m) % 2 == 0
+        return modes[m] == "O"
+
+    def meet(first, second):
+        if isinstance(second, bool):
+            return first if second else None
+        return first & second
+
     def stage_l(m):
         for i in range(prompts):
             home = t * prompts + i
-            if modes[m] != "C":
+            stays = leaves = True
+            if modes[m] == "M":
+                stays = own_line(m, z, home)
+                leaves = jnp.logical_not(stays)
+            elif modes[m] != "F":
+                stays = own_line(m, z, home)
+                leaves = not stays
+            up_line = meet(home != z, stays)
+            if up_line is not None:
                 copy = remote(
                     mine(m, i), slot(m, z), l_send.at[m, i], l_recv.at[m, z], {"sp": home}
                 )
-                begin(copy, home != z)
+                begin(copy, up_line)
+            over = meet(home != z, leaves)
             for k, peer in enumerate(x_peers):
                 device = tp_of(peer, core)
                 beside = remote(mine(m, i), slot(m, z), x_send.at[m, i, k], l_recv.at[m, z], device)
                 begin(beside, home == z)
-                if modes[m] == "D":
-                    routed = remote(
-                        mine(m, i),
-                        slot(m, z),
-                        x_send.at[m, i, k],
-                        l_recv.at[m, z],
-                        device | {"sp": home},
-                    )
-                    begin(routed, home != z)
-                elif modes[m] != "O":
+                if over is not None:
                     across = remote(
                         mine(m, i), held(m, k, i), x_send.at[m, i, k], t_recv.at[m, k, i], device
                     )
-                    begin(across, home != z)
+                    begin(across, over)
 
     def stage_t(m):
-        if modes[m] not in "FC":
+        if modes[m] == "O":
             return
         for k in range(n_x - 1):
             source = lax.rem(x + n_x - 1 - k, n_x) * CORES + core
             for i in range(prompts):
                 home = source * prompts + i
+                comes = home != z
+                if modes[m] == "M":
+                    comes = comes & jnp.logical_not(own_line(m, z, home))
                 copy = remote(
                     held(m, k, i), slot(m, z), t_send.at[m, k, i], l_recv.at[m, z], {"sp": home}
                 )
@@ -340,8 +371,8 @@
                     arrived(held(m, k, i), t_recv.at[m, k, i])
                     copy.start()
 
-                pl.when(home != z)(pass_on)
-                finish.append(lambda home=home, copy=copy: pl.when(home != z)(copy.wait_send))
+                pl.when(comes)(pass_on)
+                finish.append(lambda comes=comes, copy=copy: pl.when(comes)(copy.wait_send))
 
     owner = z // prompts
     x_in, core_in = owner // CORES, owner % CORES
@@ -351,14 +382,17 @@
 
     def enters(m, d):
         here = core == core_in
-        if d == 0 or modes[m] in "FD":
+        if d == 0 or modes[m] == "F":
             return here
-        return here & ((x == x_in) if modes[m] == "O" else (x != x_in))
+        line = own_line(m, shards[d][0], z)
+        if modes[m] == "M":
+            return here & ((x == x_in) == line)
+        return here & ((x == x_in) if line else (x != x_in))
 
     def stage_d(m, d):
         s = z if d == 0 else shards[d][0]
         copies = [partner_copy(m, d, s)]
-        if d and modes[m] in "OC":
+        if d and modes[m] != "F":
             copies += [
                 remote(slot(m, s), slot(m, s), e_send.at[m, d, k], l_recv.at[m, s], tp_of(peer, core))
                 for k, peer in enumerate(x_peers)
@@ -542,9 +576,9 @@
             pltpu.VMEM((prompts, ROPE, rows), bf16),
             pltpu.VMEM((others, prompts, ROPE, rows), bf16),
             dma((4,)),
-            dma((groups, 2)),
-            dma((units,)),
-            dma((groups, n_sp)),
+            dma((groups, 2, 2)),
+            dma((units, 2)),
+            dma((groups, n_sp, 2)),
             dma((units, peers)),
             dma((units, peers)),
             dma((units, peers)),

time: 64.7 us -> 63.7 us (0.985)
  Pallas kernels: 63 us -> 62 us
    pallas_call x1, Pallas kernels: 58.4 us -> 57.5 us  [gather_latent(): pl.pallas_call(functools.partial(gather_kernel, n_grp, n_sp, n_tp, spans,...]
where the time goes in v3:
time: 63.7 us; the launch traced here: 63.6 us
  Pallas kernels  62 us (97%)
  between operations  1.55 us (2%)
    pallas_call x1, Pallas kernels, gather_latent(): pl.pallas_call(functools.partial(gather_kernel, n_grp, n_sp, n_tp, spans,...  57.5 us
    pallas_call x1, Pallas kernels, fill_cache(): pl.pallas_call(cache_kernel, out_shape=(jax.ShapeDtypeStruct((length, out...  4.54 us

profile of v3, /device:TPU:1, one launch (start us, length us, event | category | flops | bytes accessed | tf_op | source)
XLA Modules:
  0.0 63.6 jit_solution(5558021602662719226)
XLA Ops:
  1.3 0.0 copy-start
  1.3 0.0 copy-start.1
  1.3 0.0 copy-start.2
  1.3 0.0 copy-start.3
  1.3 0.0 copy-start.4
  1.3 57.5 %shard_map.129 = (bf16[4,256,1024]{2,1,0:T(8,128)(2,1)S(1)}, bf16[4,32,256]{2,1,0:T(8,128)(2,1)S(1)}) custom-call(bf16[256,4096]{1,0:T(8,128)(2,1)} %bitcast.8, bf16[1024,1024]{1,0:T(8,128)(2,1)} %refs_1_.1, bf16[32,4096]{1,0:T(8,128)(2,1)} %bitcast.9, f32[1,4096]{1,0:T(1,128)} %bitcast.10, s32[1]{0:T(128)S(6)} %copy.14.refs_4_), custom_call_target="tpu_custom_call" | custom-call | tf_op jit(solution)/shard_map/pallas_call | solution.py:558
  58.8 0.0 copy-done
  58.8 0.0 copy-done.1
  58.8 0.0 copy-done.2
  58.8 0.0 copy-done.3
  58.8 0.0 copy-done.4
  58.9 4.5 %shard_map.130 = (bf16[1024,512]{1,0:T(8,128)(2,1)}, bf16[1024,512]{1,0:T(8,128)(2,1)}, bf16[32,1024]{1,0:T(8,128)(2,1)}, bf16[1,512]{1,0:T(2,128)(2,1)}) custom-call(bf16[4,256,1024]{2,1,0:T(8,128)(2,1)S(1)} %get-tuple-element.10.latent_ref, f32[1,1024]{1,0:T(1,128)S(1)} %bitcast.7, bf16[1024,512]{1,0:T(8,128)(2,1)S(1)} %copy-done, ...), custom_call_target="tpu_custom_call" | custom-call | tf_op jit(solution)/shard_map/pallas_call | solution.py:699
Async XLA Ops:
  1.3 57.5 %copy-start = (bf16[1024,512]{1,0:T(8,128)(2,1)S(1)}, bf16[1024,512]{1,0:T(8,128)(2,1)}, u32[]{:S(2)}) copy-start(bf16[1024,512]{1,0:T(8,128)(2,1)} %wk_ref.1) | copy-start | bytes 3145732
  1.3 57.5 %copy-start.1 = (bf16[1024,512]{1,0:T(8,128)(2,1)S(1)}, bf16[1024,512]{1,0:T(8,128)(2,1)}, u32[]{:S(2)}) copy-start(bf16[1024,512]{1,0:T(8,128)(2,1)} %wv_ref.1) | copy-start | bytes 3145732
  1.3 57.5 %copy-start.2 = (f32[1024]{0:T(1024)S(1)}, f32[1024]{0:T(1024)}, u32[]{:S(2)}) copy-start(f32[1024]{0:T(1024)} %param.15) | copy-start | bytes 12292
  1.3 57.5 %copy-start.3 = (bf16[1,512]{1,0:T(2,128)(2,1)S(1)}, bf16[1,512]{1,0:T(2,128)(2,1)}, u32[]{:S(2)}) copy-start(bf16[1,512]{1,0:T(2,128)(2,1)} %q_nope_ref.1) | copy-start | bytes 3076
  1.3 57.5 %copy-start.4 = (bf16[1,256]{1,0:T(2,128)(2,1)S(1)}, bf16[1,256]{1,0:T(2,128)(2,1)}, u32[]{:S(2)}) copy-start(bf16[1,256]{1,0:T(2,128)(2,1)} %q_rope_ref.1) | copy-start | bytes 1540

commit v4 on v3

--- a/solution.py
+++ b/solution.py
@@ -14,75 +14,79 @@
 PIECES = 4
 PENDING = 60
 PARTS = (1, 1, 1, 1, 1, 1, 1, 1)
-MODES = ("M", "F", "M", "M", "F", "M", "F", "O", "F")
-DOUBLED = (False, False, False, False, True, False, True, True)
-X_FIRST = (False, True, True, True, True, True, True, False, True, False, True, True, False, False, True, False, True, True, False, False, True, False, True, True)
+MODES = ("M", "C", "C", "O", "O", "C", "C", "O", "O")
+DOUBLED = (False, False, False, False, True, True, True, True)
+X_FIRST = (True, False, True, False, True, True, True, False, False, True, True, True, True, False, False, True, True, True, False, False, False, False, False, False)
 OUTER = (
-    ("own", 2), ("norm", 1), ("own", 0), ("own", 1), ("norm", 2), ("norm", 0), ("norm", 3),
-    ("odot", 0), ("odot", 5), ("a", 3), ("a", 6), ("a", 0), ("odot", 6), ("odot", 1), ("odot", 2),
-    ("odot", 7), ("odot", 3), ("own", 3), ("own", 4), ("b", 3), ("b", 6), ("b", 0), ("a", 7),
-    ("own", 5), ("a", 1), ("a", 9), ("a", 4), ("c", 0), ("a", 2), ("odot", 4), ("own", 6), ("l", 0),
-    ("a", 12), ("b", 1), ("b", 9), ("b", 4), ("own", 7), ("a", 5), ("c", 3), ("a", 10), ("a", 8),
-    ("a", 15), ("c", 6), ("dot", 0), ("dot", 3), ("b", 7), ("c", 9), ("b", 2), ("t", 0), ("a", 13),
-    ("b", 13), ("c", 1), ("a", 11), ("b", 12), ("c", 12), ("c", 4), ("d", 0, 2), ("dot", 6),
-    ("dot", 9), ("a", 18), ("b", 10), ("d", 0, 0), ("b", 15), ("b", 5), ("dot", 1), ("d", 0, 1),
-    ("b", 18), ("dot", 12), ("b", 8), ("dot", 4), ("c", 7), ("a", 14), ("c", 2), ("a", 16),
-    ("dot", 7), ("d", 0, 3), ("b", 11), ("e", 0, 2), ("c", 13), ("dot", 13), ("a", 21), ("a", 19),
-    ("c", 10), ("a", 17), ("c", 15), ("dot", 2), ("l", 1), ("b", 16), ("e", 0, 3), ("e", 0, 1),
-    ("c", 5), ("b", 21), ("c", 8), ("a", 22), ("dot", 10), ("dot", 5), ("l", 2), ("c", 11),
-    ("dot", 8), ("l", 3), ("dot", 15), ("a", 20), ("c", 18), ("t", 1), ("b", 17), ("c", 21),
-    ("dot", 18), ("b", 14), ("c", 14), ("dot", 11), ("l", 4), ("b", 20), ("t", 3), ("a", 23),
-    ("dot", 14), ("l", 5), ("b", 19), ("c", 19), ("c", 20), ("d", 3, 0), ("dot", 21), ("t", 2),
-    ("c", 16), ("dot", 16), ("c", 17), ("d", 2, 2), ("d", 2, 0), ("dot", 20), ("b", 23), ("c", 23),
-    ("d", 1, 1), ("t", 5), ("t", 4), ("dot", 19), ("l", 7), ("d", 1, 0), ("d", 4, 0), ("d", 3, 3),
-    ("dot", 17), ("l", 6), ("dot", 23), ("d", 5, 0), ("d", 2, 3), ("d", 1, 2), ("b", 22), ("c", 22),
-    ("d", 5, 3), ("d", 2, 1), ("e", 2, 2), ("dot", 22), ("l", 8), ("d", 3, 1), ("d", 5, 1),
-    ("d", 5, 2), ("d", 4, 1), ("d", 3, 2), ("e", 3, 1), ("e", 3, 3), ("d", 1, 3), ("d", 7, 3),
-    ("e", 2, 1), ("d", 4, 3), ("d", 4, 2), ("d", 7, 0), ("d", 7, 2), ("t", 6), ("d", 6, 1),
-    ("d", 6, 2), ("d", 7, 1), ("d", 6, 3), ("d", 6, 0), ("e", 7, 3), ("e", 5, 1), ("e", 2, 3),
-    ("t", 8), ("e", 7, 1), ("e", 5, 3), ("e", 3, 2), ("e", 5, 2), ("d", 8, 1), ("e", 7, 2),
-    ("d", 8, 0), ("d", 8, 2), ("d", 8, 3), ("end", 0, 0), ("end", 0, 1), ("end", 0, 2),
-    ("end", 0, 3), ("end", 1, 0), ("end", 1, 1), ("end", 1, 2), ("end", 1, 3), ("end", 2, 0),
-    ("end", 2, 1), ("end", 2, 2), ("end", 2, 3), ("end", 3, 0), ("end", 3, 1), ("end", 3, 2),
-    ("end", 3, 3), ("end", 4, 0), ("end", 4, 1), ("end", 4, 2), ("end", 4, 3), ("end", 5, 0),
-    ("end", 5, 1), ("end", 5, 2), ("end", 5, 3), ("end", 6, 0), ("end", 6, 1), ("end", 6, 2),
-    ("end", 6, 3), ("end", 7, 0), ("end", 7, 1), ("end", 7, 2), ("end", 7, 3), ("end", 8, 0),
-    ("end", 8, 1), ("end", 8, 2), ("end", 8, 3),
+    ("own", 0), ("norm", 0), ("own", 1), ("norm", 1), ("norm", 2), ("own", 2), ("norm", 3),
+    ("odot", 0), ("odot", 1), ("odot", 2), ("odot", 4), ("odot", 6), ("own", 3), ("odot", 5),
+    ("odot", 7), ("odot", 3), ("a", 3), ("a", 0), ("a", 6), ("own", 5), ("a", 1), ("b", 0),
+    ("a", 9), ("own", 4), ("b", 6), ("b", 3), ("a", 4), ("a", 7), ("c", 0), ("a", 2), ("b", 9),
+    ("b", 1), ("a", 12), ("b", 12), ("l", 0), ("a", 5), ("a", 10), ("own", 6), ("c", 6), ("b", 4),
+    ("dot", 0), ("a", 8), ("dot", 6), ("b", 7), ("a", 15), ("c", 1), ("b", 2), ("own", 7),
+    ("a", 18), ("b", 18), ("c", 12), ("c", 3), ("a", 13), ("b", 5), ("dot", 3), ("t", 0),
+    ("dot", 12), ("c", 4), ("c", 9), ("b", 10), ("dot", 1), ("b", 8), ("a", 16), ("c", 2),
+    ("dot", 9), ("a", 11), ("b", 13), ("c", 7), ("dot", 7), ("c", 13), ("a", 21), ("a", 14),
+    ("b", 14), ("dot", 2), ("l", 1), ("d", 0, 2), ("a", 19), ("b", 15), ("c", 15), ("dot", 4),
+    ("c", 18), ("c", 5), ("dot", 13), ("d", 0, 0), ("b", 16), ("c", 16), ("b", 11), ("c", 10),
+    ("c", 8), ("dot", 18), ("a", 22), ("b", 22), ("dot", 5), ("l", 2), ("a", 17), ("dot", 10),
+    ("d", 0, 3), ("dot", 8), ("l", 3), ("c", 14), ("dot", 16), ("d", 0, 1), ("a", 20), ("b", 20),
+    ("dot", 15), ("t", 1), ("d", 1, 0), ("a", 23), ("c", 11), ("b", 19), ("c", 19), ("c", 22),
+    ("dot", 14), ("l", 5), ("dot", 11), ("l", 4), ("b", 23), ("dot", 19), ("t", 2), ("b", 17),
+    ("c", 17), ("d", 2, 0), ("dot", 22), ("b", 21), ("c", 21), ("e", 0, 2), ("e", 0, 3),
+    ("dot", 17), ("l", 6), ("d", 1, 2), ("c", 20), ("dot", 21), ("e", 0, 1), ("c", 23), ("d", 3, 0),
+    ("d", 1, 3), ("d", 4, 0), ("d", 3, 1), ("d", 3, 2), ("dot", 20), ("l", 7), ("d", 3, 3),
+    ("d", 2, 3), ("t", 5), ("d", 5, 0), ("d", 5, 1), ("d", 5, 2), ("dot", 23), ("l", 8),
+    ("d", 8, 1), ("d", 2, 1), ("d", 7, 2), ("d", 2, 2), ("e", 2, 3), ("t", 6), ("d", 6, 0),
+    ("d", 7, 1), ("d", 4, 3), ("d", 1, 1), ("e", 1, 2), ("d", 6, 1), ("d", 5, 3), ("e", 5, 2),
+    ("d", 6, 2), ("d", 4, 2), ("d", 4, 1), ("e", 3, 2), ("e", 5, 1), ("d", 6, 3), ("e", 3, 1),
+    ("d", 7, 0), ("e", 3, 3), ("e", 2, 1), ("e", 1, 3), ("e", 2, 2), ("d", 8, 0), ("d", 7, 3),
+    ("e", 7, 2), ("e", 4, 2), ("e", 4, 1), ("e", 7, 1), ("d", 8, 2), ("d", 8, 3), ("e", 1, 1),
+    ("e", 6, 1), ("e", 4, 3), ("e", 5, 3), ("e", 8, 1), ("e", 7, 3), ("e", 6, 2), ("e", 8, 2),
+    ("e", 8, 3), ("e", 6, 3), ("end", 0, 0), ("end", 0, 1), ("end", 0, 2), ("end", 0, 3),
+    ("end", 1, 0), ("end", 1, 1), ("end", 1, 2), ("end", 1, 3), ("end", 2, 0), ("end", 2, 1),
+    ("end", 2, 2), ("end", 2, 3), ("end", 3, 0), ("end", 3, 1), ("end", 3, 2), ("end", 3, 3),
+    ("end", 4, 0), ("end", 4, 1), ("end", 4, 2), ("end", 4, 3), ("end", 5, 0), ("end", 5, 1),
+    ("end", 5, 2), ("end", 5, 3), ("end", 6, 0), ("end", 6, 1), ("end", 6, 2), ("end", 6, 3),
+    ("end", 7, 0), ("end", 7, 1), ("end", 7, 2), ("end", 7, 3), ("end", 8, 0), ("end", 8, 1),
+    ("end", 8, 2), ("end", 8, 3),
 )
 MIDDLE = (
-    ("own", 0), ("norm", 0), ("own", 1), ("norm", 1), ("own", 2), ("norm", 2), ("norm", 3),
-    ("z", 6), ("z", 1), ("z", 0), ("own", 3), ("z", 4), ("z", 3), ("z", 7), ("a", 1), ("odot", 5),
-    ("odot", 0), ("a", 3), ("odot", 1), ("odot", 2), ("a", 0), ("odot", 4), ("odot", 7), ("own", 4),
-    ("a", 6), ("odot", 3), ("odot", 6), ("z", 2), ("b", 1), ("b", 0), ("z", 9), ("b", 3), ("z", 5),
-    ("a", 7), ("a", 2), ("l", 0), ("own", 5), ("z", 10), ("z", 8), ("a", 4), ("a", 9), ("c", 1),
-    ("c", 0), ("a", 5), ("z", 13), ("z", 12), ("a", 10), ("a", 12), ("b", 12), ("a", 8), ("a", 13),
-    ("b", 13), ("b", 6), ("z", 11), ("own", 6), ("c", 3), ("t", 0), ("d", 0, 0), ("b", 7),
-    ("z", 15), ("b", 2), ("a", 11), ("dot", 3), ("b", 4), ("z", 16), ("own", 7), ("dot", 1),
-    ("dot", 0), ("b", 9), ("c", 6), ("b", 5), ("d", 0, 3), ("z", 14), ("a", 16), ("c", 7), ("c", 4),
-    ("c", 2), ("b", 10), ("z", 21), ("a", 15), ("z", 19), ("b", 8), ("c", 12), ("c", 13), ("z", 17),
-    ("a", 14), ("b", 14), ("b", 11), ("dot", 4), ("z", 22), ("a", 17), ("c", 9), ("d", 0, 2),
-    ("z", 18), ("a", 19), ("b", 19), ("a", 18), ("dot", 7), ("dot", 2), ("l", 1), ("c", 10),
-    ("d", 0, 1), ("z", 20), ("b", 15), ("dot", 13), ("c", 5), ("dot", 9), ("b", 16), ("b", 18),
-    ("dot", 12), ("e", 0, 3), ("dot", 5), ("l", 2), ("dot", 6), ("c", 8), ("a", 22), ("a", 20),
-    ("b", 20), ("t", 1), ("e", 0, 2), ("c", 14), ("c", 11), ("a", 21), ("z", 23), ("a", 23),
-    ("c", 19), ("b", 21), ("b", 17), ("dot", 10), ("c", 18), ("dot", 8), ("l", 3), ("dot", 14),
-    ("l", 5), ("c", 16), ("b", 22), ("e", 0, 1), ("c", 15), ("dot", 11), ("l", 4), ("dot", 19),
-    ("b", 23), ("c", 21), ("c", 22), ("c", 23), ("t", 3), ("dot", 15), ("c", 20), ("dot", 16),
-    ("c", 17), ("dot", 21), ("d", 3, 3), ("d", 3, 0), ("t", 2), ("d", 2, 0), ("d", 2, 1),
-    ("d", 2, 3), ("dot", 20), ("dot", 18), ("l", 7), ("d", 3, 2), ("dot", 17), ("l", 6),
-    ("d", 3, 1), ("t", 4), ("d", 4, 0), ("d", 1, 2), ("d", 1, 0), ("d", 2, 2), ("e", 2, 3),
-    ("dot", 22), ("t", 5), ("d", 5, 0), ("d", 1, 1), ("d", 7, 0), ("d", 1, 3), ("d", 5, 2),
-    ("dot", 23), ("l", 8), ("d", 5, 1), ("d", 4, 2), ("d", 4, 1), ("e", 3, 1), ("d", 7, 1),
-    ("e", 2, 2), ("e", 3, 2), ("e", 2, 1), ("d", 5, 3), ("t", 6), ("d", 6, 1), ("d", 7, 3),
-    ("t", 8), ("d", 7, 2), ("e", 7, 1), ("e", 7, 3), ("d", 6, 2), ("e", 5, 3), ("e", 3, 3),
-    ("d", 4, 3), ("e", 5, 2), ("e", 5, 1), ("d", 6, 3), ("d", 6, 0), ("e", 7, 2), ("d", 8, 2),
-    ("d", 8, 1), ("d", 8, 3), ("d", 8, 0), ("end", 0, 0), ("end", 0, 1), ("end", 0, 2),
-    ("end", 0, 3), ("end", 1, 0), ("end", 1, 1), ("end", 1, 2), ("end", 1, 3), ("end", 2, 0),
-    ("end", 2, 1), ("end", 2, 2), ("end", 2, 3), ("end", 3, 0), ("end", 3, 1), ("end", 3, 2),
-    ("end", 3, 3), ("end", 4, 0), ("end", 4, 1), ("end", 4, 2), ("end", 4, 3), ("end", 5, 0),
-    ("end", 5, 1), ("end", 5, 2), ("end", 5, 3), ("end", 6, 0), ("end", 6, 1), ("end", 6, 2),
-    ("end", 6, 3), ("end", 7, 0), ("end", 7, 1), ("end", 7, 2), ("end", 7, 3), ("end", 8, 0),
-    ("end", 8, 1), ("end", 8, 2), ("end", 8, 3),
+    ("own", 1), ("norm", 1), ("own", 0), ("norm", 0), ("own", 2), ("norm", 2), ("norm", 3),
+    ("z", 0), ("z", 1), ("a", 0), ("z", 4), ("own", 3), ("odot", 1), ("a", 1), ("odot", 0),
+    ("odot", 2), ("odot", 3), ("a", 4), ("z", 3), ("odot", 5), ("odot", 6), ("odot", 7),
+    ("odot", 4), ("own", 4), ("a", 3), ("b", 0), ("z", 7), ("a", 7), ("z", 6), ("z", 2), ("a", 2),
+    ("l", 0), ("b", 1), ("z", 10), ("z", 9), ("z", 5), ("b", 4), ("own", 5), ("a", 6), ("z", 8),
+    ("a", 8), ("a", 10), ("b", 3), ("b", 2), ("c", 0), ("a", 5), ("a", 9), ("b", 7), ("own", 6),
+    ("z", 13), ("z", 16), ("a", 13), ("b", 13), ("b", 10), ("z", 11), ("z", 12), ("a", 12),
+    ("b", 12), ("b", 6), ("z", 15), ("a", 15), ("b", 15), ("own", 7), ("c", 4), ("c", 1),
+    ("dot", 1), ("z", 14), ("z", 18), ("a", 18), ("c", 13), ("b", 8), ("dot", 0), ("z", 19),
+    ("b", 5), ("c", 3), ("c", 2), ("a", 11), ("a", 16), ("b", 16), ("c", 15), ("b", 9), ("dot", 4),
+    ("z", 22), ("b", 18), ("c", 7), ("c", 12), ("a", 14), ("c", 6), ("a", 22), ("dot", 3),
+    ("dot", 2), ("l", 1), ("z", 21), ("c", 18), ("dot", 18), ("a", 19), ("b", 19), ("t", 0),
+    ("c", 10), ("z", 17), ("z", 20), ("a", 17), ("b", 17), ("dot", 7), ("d", 0, 0), ("a", 21),
+    ("b", 21), ("dot", 12), ("c", 5), ("c", 16), ("b", 22), ("b", 11), ("dot", 13), ("b", 14),
+    ("a", 20), ("b", 20), ("dot", 15), ("c", 14), ("z", 23), ("c", 9), ("dot", 9), ("c", 22),
+    ("a", 23), ("b", 23), ("c", 8), ("dot", 5), ("l", 2), ("t", 1), ("d", 1, 0), ("c", 17),
+    ("c", 19), ("dot", 22), ("c", 21), ("dot", 14), ("l", 5), ("dot", 10), ("dot", 16), ("dot", 6),
+    ("c", 20), ("c", 11), ("dot", 8), ("l", 3), ("dot", 17), ("l", 6), ("d", 1, 1), ("c", 23),
+    ("d", 3, 0), ("d", 1, 2), ("dot", 20), ("dot", 19), ("l", 7), ("d", 1, 3), ("dot", 21),
+    ("dot", 11), ("l", 4), ("d", 0, 2), ("d", 0, 1), ("t", 5), ("d", 5, 0), ("d", 0, 3),
+    ("e", 0, 3), ("dot", 23), ("l", 8), ("t", 2), ("d", 2, 0), ("d", 2, 3), ("d", 3, 2),
+    ("d", 2, 1), ("t", 6), ("d", 3, 1), ("d", 3, 3), ("d", 4, 0), ("e", 3, 3), ("e", 1, 1),
+    ("e", 1, 2), ("d", 7, 0), ("d", 2, 2), ("d", 6, 0), ("d", 4, 3), ("d", 7, 2), ("d", 4, 2),
+    ("e", 2, 3), ("d", 4, 1), ("d", 7, 3), ("e", 0, 2), ("d", 7, 1), ("e", 3, 1), ("d", 5, 2),
+    ("e", 3, 2), ("e", 4, 3), ("d", 5, 1), ("d", 8, 0), ("e", 7, 2), ("e", 2, 2), ("d", 5, 3),
+    ("e", 1, 3), ("d", 8, 3), ("d", 6, 2), ("d", 8, 2), ("d", 8, 1), ("e", 4, 2), ("e", 2, 1),
+    ("e", 4, 1), ("e", 5, 3), ("e", 0, 1), ("d", 6, 1), ("e", 5, 2), ("d", 6, 3), ("e", 6, 2),
+    ("e", 6, 1), ("e", 7, 3), ("e", 7, 1), ("e", 5, 1), ("e", 8, 3), ("e", 6, 3), ("e", 8, 2),
+    ("e", 8, 1), ("end", 0, 0), ("end", 0, 1), ("end", 0, 2), ("end", 0, 3), ("end", 1, 0),
+    ("end", 1, 1), ("end", 1, 2), ("end", 1, 3), ("end", 2, 0), ("end", 2, 1), ("end", 2, 2),
+    ("end", 2, 3), ("end", 3, 0), ("end", 3, 1), ("end", 3, 2), ("end", 3, 3), ("end", 4, 0),
+    ("end", 4, 1), ("end", 4, 2), ("end", 4, 3), ("end", 5, 0), ("end", 5, 1), ("end", 5, 2),
+    ("end", 5, 3), ("end", 6, 0), ("end", 6, 1), ("end", 6, 2), ("end", 6, 3), ("end", 7, 0),
+    ("end", 7, 1), ("end", 7, 2), ("end", 7, 3), ("end", 8, 0), ("end", 8, 1), ("end", 8, 2),
+    ("end", 8, 3),
 )
 
 EPS = 1e-06

time: 63.7 us -> 62.4 us (0.980)
  Pallas kernels: 62 us -> 60.7 us
    pallas_call x1, Pallas kernels: 57.5 us -> 56.1 us  [gather_latent(): pl.pallas_call(functools.partial(gather_kernel, n_grp, n_sp, n_tp, spans,...]
where the time goes in v4:
time: 62.4 us; the launch traced here: 62.2 us
  Pallas kernels  60.7 us (97%)
  between operations  1.55 us (2%)
    pallas_call x1, Pallas kernels, gather_latent(): pl.pallas_call(functools.partial(gather_kernel, n_grp, n_sp, n_tp, spans,...  56.1 us
    pallas_call x1, Pallas kernels, fill_cache(): pl.pallas_call(cache_kernel, out_shape=(jax.ShapeDtypeStruct((length, out...  4.54 us

profile of v4, /device:TPU:1, one launch (start us, length us, event | category | flops | bytes accessed | tf_op | source)
XLA Modules:
  0.0 62.2 jit_solution(9811391675939522824)
XLA Ops:
  1.3 0.0 copy-start
  1.3 0.0 copy-start.1
  1.3 0.0 copy-start.2
  1.3 0.0 copy-start.3
  1.3 0.0 copy-start.4
  1.3 56.1 %shard_map.129 = (bf16[4,256,1024]{2,1,0:T(8,128)(2,1)S(1)}, bf16[4,32,256]{2,1,0:T(8,128)(2,1)S(1)}) custom-call(bf16[256,4096]{1,0:T(8,128)(2,1)} %bitcast.8, bf16[1024,1024]{1,0:T(8,128)(2,1)} %refs_1_.1, bf16[32,4096]{1,0:T(8,128)(2,1)} %bitcast.9, f32[1,4096]{1,0:T(1,128)} %bitcast.10, s32[1]{0:T(128)S(6)} %copy.14.refs_4_), custom_call_target="tpu_custom_call" | custom-call | tf_op jit(solution)/shard_map/pallas_call | solution.py:562
  57.5 0.0 copy-done
  57.5 0.0 copy-done.1
  57.5 0.0 copy-done.2
  57.5 0.0 copy-done.3
  57.5 0.0 copy-done.4
  57.5 4.5 %shard_map.130 = (bf16[1024,512]{1,0:T(8,128)(2,1)}, bf16[1024,512]{1,0:T(8,128)(2,1)}, bf16[32,1024]{1,0:T(8,128)(2,1)}, bf16[1,512]{1,0:T(2,128)(2,1)}) custom-call(bf16[4,256,1024]{2,1,0:T(8,128)(2,1)S(1)} %get-tuple-element.10.latent_ref, f32[1,1024]{1,0:T(1,128)S(1)} %bitcast.7, bf16[1024,512]{1,0:T(8,128)(2,1)S(1)} %copy-done, ...), custom_call_target="tpu_custom_call" | custom-call | tf_op jit(solution)/shard_map/pallas_call | solution.py:703
Async XLA Ops:
  1.3 56.2 %copy-start = (bf16[1024,512]{1,0:T(8,128)(2,1)S(1)}, bf16[1024,512]{1,0:T(8,128)(2,1)}, u32[]{:S(2)}) copy-start(bf16[1024,512]{1,0:T(8,128)(2,1)} %wk_ref.1) | copy-start | bytes 3145732
  1.3 56.2 %copy-start.1 = (bf16[1024,512]{1,0:T(8,128)(2,1)S(1)}, bf16[1024,512]{1,0:T(8,128)(2,1)}, u32[]{:S(2)}) copy-start(bf16[1024,512]{1,0:T(8,128)(2,1)} %wv_ref.1) | copy-start | bytes 3145732
  1.3 56.2 %copy-start.2 = (f32[1024]{0:T(1024)S(1)}, f32[1024]{0:T(1024)}, u32[]{:S(2)}) copy-start(f32[1024]{0:T(1024)} %param.15) | copy-start | bytes 12292
  1.3 56.2 %copy-start.3 = (bf16[1,512]{1,0:T(2,128)(2,1)S(1)}, bf16[1,512]{1,0:T(2,128)(2,1)}, u32[]{:S(2)}) copy-start(bf16[1,512]{1,0:T(2,128)(2,1)} %q_nope_ref.1) | copy-start | bytes 3076
  1.3 56.2 %copy-start.4 = (bf16[1,256]{1,0:T(2,128)(2,1)S(1)}, bf16[1,256]{1,0:T(2,128)(2,1)}, u32[]{:S(2)}) copy-start(bf16[1,256]{1,0:T(2,128)(2,1)} %q_rope_ref.1) | copy-start | bytes 1540
